TPU v7x, 32 devices: a whole 2x2x4 slice. The times are simulated.
32 devices in a mesh: ep: 8 (over z, core), tp: 4 (over y, x).
Axes of the slice: x: 2, y: 2, z: 4, core: 2. Of those that a mesh axis runs over, the one named last changes fastest.
Arguments:
- tokens: bfloat16 [128, 2048], P('ep'), may hold values from -6 to 6
- attn_gain: float32 [2048], replicated, may hold values from 0.1 to 1.9
- query_weight: bfloat16 [2048, 2048], P('ep', 'tp'), may hold values from -0.125 to 0.125
- key_weight: bfloat16 [2048, 2048], P('ep', 'tp'), may hold values from -0.125 to 0.125
- value_weight: bfloat16 [2048, 2048], P('ep', 'tp'), may hold values from -0.125 to 0.125
- forget_weight: bfloat16 [2048, 16], P(None, 'tp'), may hold values from -0.125 to 0.125
- forget_bias: float32 [16], P('tp'), may hold values from -1 to 2
- cache_keys: bfloat16 [128, 16, 384, 128], P('ep', 'tp'), may hold values from -240 to 240
- cache_values: bfloat16 [128, 16, 384, 128], P('ep', 'tp'), may hold values from -6 to 6
- cache_gates: float32 [128, 16, 384], P('ep', 'tp'), may hold values from -768 to 0, as said below
- lengths: int32 [128], P('ep'), may hold values from 1 to 384
- output_weight: bfloat16 [2048, 2048], P('tp', 'ep'), may hold values from -0.125 to 0.125
- ffn_gain: float32 [2048], replicated, may hold values from 0.1 to 1.9
- dense_gate_proj: bfloat16 [2048, 2048], P('ep', 'tp'), may hold values from -0.125 to 0.125
- dense_up_proj: bfloat16 [2048, 2048], P('ep', 'tp'), may hold values from -0.125 to 0.125
- dense_down_proj: bfloat16 [2048, 2048], P('tp', 'ep'), may hold values from -0.125 to 0.125
- dense_mix: bfloat16 [2048], replicated, may hold values from -0.125 to 0.125
- expert_ids: int32 [128, 2], P('ep'), may hold values from 0 to 7, as said below
- group_prob: float32 [128], P('ep'), may hold values from 0.25 to 1
- pair_prob: float32 [128, 2], P('ep'), may hold values from 0.05 to 1
- expert_gate: bfloat16 [8, 2048, 2048], P('ep', None, 'tp'), may hold values from -0.125 to 0.125
- expert_up: bfloat16 [8, 2048, 2048], P('ep', None, 'tp'), may hold values from -0.125 to 0.125
- expert_down: bfloat16 [8, 2048, 2048], P('ep', 'tp'), may hold values from -0.125 to 0.125
Outputs:
- mixed_out: bfloat16 [128, 2048], P('ep')
Inputs may be any that keep to these rules, and one draw needn't show every extreme that they name: `expert_ids`: each row names two different experts of one group, the groups being 4 runs of consecutive ids. In each aligned block of 16 rows (the rows of one index of ep) no expert is named more than 8 times, and some expert exactly 8 times. `cache_gates`: along positions the values never rise.
All inputs are finite; a program needn't handle non-finite values.
Results may differ from a plain program's by a relative error of at most 0.014.
Values may be sent and summed in bfloat16 or wider, within the bound.
A program may use at most 64 MiB of HBM per device.

v0:
```python
import functools
import math

import jax
import jax.numpy as jnp
from jax import lax
from jax.experimental import pallas as pl
from jax.experimental.pallas import tpu as pltpu
from jax.sharding import PartitionSpec as P

EPSILON = 1e-06


def rms_scale(values, norm_gain):
    widened = values.astype(jnp.float32)
    return (
        widened
        * lax.rsqrt(jnp.mean(widened * widened, axis=-1, keepdims=True) + EPSILON)
        * norm_gain
    )


MESH = pl.DeviceIdType.MESH
F32 = jnp.float32
BF16 = jnp.bfloat16


def fan_out(axis, count, me, source_of, landing, send_sem, recv_sem, slot=None):
    copies = []
    place = me if slot is None else slot(me)
    for step in range(1, count):
        target = lax.rem(me + step, count)
        copy = pltpu.make_async_remote_copy(
            src_ref=source_of(target),
            dst_ref=landing.at[place],
            send_sem=send_sem.at[step],
            recv_sem=recv_sem.at[me],
            device_id={axis: target},
            device_id_type=MESH,
        )
        copy.start()
        copies.append(copy)
    return copies


def collect(axis, count, me, landing, send_sem, recv_sem, slot=None):
    for step in range(1, count):
        source = lax.rem(me + count - step, count)
        place = source if slot is None else slot(source)
        pltpu.make_async_remote_copy(
            src_ref=landing.at[place],
            dst_ref=landing.at[place],
            send_sem=send_sem.at[step],
            recv_sem=recv_sem.at[source],
            device_id={axis: source},
            device_id_type=MESH,
        ).wait_recv()


def spread_rows(axis_ep, axis_tp, n_ep, n_tp, me_ep, me_tp, held, landing, send_sem, recv_sem):
    ratio = n_ep // n_tp
    for part in range(ratio):
        target_ep = me_tp * ratio + part
        for step in range(n_tp):
            target_tp = lax.rem(me_tp + step, n_tp)

            def send():
                pltpu.make_async_remote_copy(
                    src_ref=held.at[part],
                    dst_ref=landing.at[me_ep],
                    send_sem=send_sem.at[part * n_tp + step],
                    recv_sem=recv_sem.at[me_ep],
                    device_id={axis_ep: target_ep, axis_tp: target_tp},
                    device_id_type=MESH,
                ).start()

            if step == 0:
                pl.when(target_ep != me_ep)(send)

                @pl.when(target_ep == me_ep)
                def _():
                    landing[me_ep] = held[part]
            else:
                send()


def spread_wait(axis_ep, axis_tp, n_ep, n_tp, me_ep, me_tp, held, landing, send_sem, recv_sem):
    ratio = n_ep // n_tp
    own_tp = me_ep // ratio
    for step in range(n_ep):
        source = lax.rem(me_ep + n_ep - step, n_ep)

        def arrive():
            pltpu.make_async_remote_copy(
                src_ref=landing.at[source],
                dst_ref=landing.at[source],
                send_sem=send_sem.at[0],
                recv_sem=recv_sem.at[source],
                device_id={axis_ep: source, axis_tp: own_tp},
                device_id_type=MESH,
            ).wait_recv()

        if step == 0:
            pl.when(own_tp != me_tp)(arrive)
        else:
            arrive()


def spread_sent(axis_ep, axis_tp, n_ep, n_tp, me_ep, me_tp, held, landing, send_sem, recv_sem):
    ratio = n_ep // n_tp
    for part in range(ratio):
        target_ep = me_tp * ratio + part
        for step in range(n_tp):
            target_tp = lax.rem(me_tp + step, n_tp)

            def sent():
                pltpu.make_async_remote_copy(
                    src_ref=held.at[part],
                    dst_ref=landing.at[me_ep],
                    send_sem=send_sem.at[part * n_tp + step],
                    recv_sem=recv_sem.at[me_ep],
                    device_id={axis_ep: target_ep, axis_tp: target_tp},
                    device_id_type=MESH,
                ).wait_send()

            if step == 0:
                pl.when(target_ep != me_ep)(sent)
            else:
                sent()


def total_of(ref, count):
    total = ref[0].astype(F32)
    for index in range(1, count):
        total = total + ref[index].astype(F32)
    return total


def dot32(left, right):
    return jnp.dot(left, right, preferred_element_type=F32)


def chip_order(index, half):
    return lax.rem(index, 2) * half + index // 2


def pair_copy(axis, me, source, landing, send_sem, recv_sem, slot):
    return pltpu.make_async_remote_copy(
        src_ref=source,
        dst_ref=landing,
        send_sem=send_sem.at[slot],
        recv_sem=recv_sem.at[slot],
        device_id={axis: me + 1 - 2 * lax.rem(me, 2)},
        device_id_type=MESH,
    )


def chip_fan(axis, half, me, held, landing, send_sem, recv_sem):
    chip, core = me // 2, lax.rem(me, 2)
    copies = []
    for step in range(1, half):
        target = lax.rem(chip + step, half)
        copy = pltpu.make_async_remote_copy(
            src_ref=held.at[target],
            dst_ref=landing.at[chip],
            send_sem=send_sem.at[step],
            recv_sem=recv_sem.at[chip],
            device_id={axis: target * 2 + core},
            device_id_type=MESH,
        )
        copy.start()
        copies.append(copy)
    landing[chip] = held[chip]
    return copies


def chip_collect(axis, half, me, landing, send_sem, recv_sem):
    chip, core = me // 2, lax.rem(me, 2)
    for step in range(1, half):
        source = lax.rem(chip + half - step, half)
        pltpu.make_async_remote_copy(
            src_ref=landing.at[source],
            dst_ref=landing.at[source],
            send_sem=send_sem.at[step],
            recv_sem=recv_sem.at[source],
            device_id={axis: source * 2 + core},
            device_id_type=MESH,
        ).wait_recv()


def layer_kernel(
    n_ep,
    n_tp,
    forget_bias,
    lengths,
    tokens,
    attn_gain,
    forget_rows,
    gates,
    gain,
    gain_parts,
    dense_mix,
    to_slots,
    from_first,
    from_second,
    routes,
    query_weight,
    key_weight,
    value_weight,
    keys,
    values,
    output_weight,
    dense_gate,
    dense_up,
    expert_gate,
    expert_up,
    expert_down,
    dense_down,
    out,
    query_weight_held,
    key_weight_held,
    value_weight_held,
    keys_held,
    values_held,
    output_weight_held,
    dense_gate_held,
    dense_up_held,
    expert_gate_held,
    expert_up_held,
    expert_down_held,
    dense_down_held,
    load_sem,
    norm_send,
    norm_land,
    norm_ss,
    norm_rs,
    part_send,
    part_land,
    part_ss,
    part_rs,
    score_send,
    score_land,
    score_ss,
    score_rs,
    value_send,
    value_land,
    value_ss,
    value_rs,
    query_rows,
    key_rows,
    value_rows,
    forget_logs,
    scores,
    mixed,
    attended,
    full,
    att_land,
    att_ss,
    att_rs,
    head_send,
    head_land,
    head_ss,
    head_rs,
    mix_send,
    mix_land,
    mix_ss,
    mix_rs,
    token_send,
    token_land,
    token_ss,
    token_rs,
    share_land,
    share_ss,
    share_rs,
    slot_send,
    slot_land,
    slot_ss,
    slot_rs,
    pair_send,
    pair_land,
    pair_ss,
    pair_rs,
    dense_send,
    dense_land,
    dense_ss,
    dense_rs,
    expert_send,
    expert_land,
    expert_ss,
    expert_rs,
    back_send,
    back_land,
    back_ss,
    back_rs,
    hidden_send,
    hidden_land,
    hidden_ss,
    hidden_rs,
    down_send,
    down_land,
    down_ss,
    down_rs,
    tail_send,
    tail_land,
    tail_ss,
    tail_rs,
    route_send,
    route_land,
    route_ss,
    route_rs,
):
    me = lax.axis_index("ep")
    me_tp = lax.axis_index("tp")
    barrier = pltpu.get_barrier_semaphore()
    everyone = n_ep * n_tp
    place = me * n_tp + me_tp

    def greet(step, carry):
        other = lax.rem(place + step, everyone)
        pl.semaphore_signal(
            barrier,
            inc=1,
            device_id={"ep": other // n_tp, "tp": lax.rem(other, n_tp)},
            device_id_type=MESH,
        )
        return carry

    lax.fori_loop(1, everyone, greet, 0)
    sources = (query_weight, key_weight, value_weight, keys, values, output_weight, dense_gate, dense_up, expert_gate, expert_up, expert_down, dense_down)
    places = (query_weight_held, key_weight_held, value_weight_held, keys_held, values_held, output_weight_held, dense_gate_held, dense_up_held, expert_gate_held, expert_up_held, expert_down_held, dense_down_held)
    loads = [
        pltpu.make_async_copy(source, place, load_sem.at[index])
        for index, (source, place) in enumerate(zip(sources, places))
    ]
    for load in loads:
        load.start()
    rows, model = tokens.shape
    depth, hidden = query_weight.shape
    heads, span, size = keys.shape[1:]
    slots = slot_send.shape[1]
    group_rows = n_ep * rows // n_tp
    ratio = n_ep // n_tp
    half = n_ep // 2
    chip, core = me // 2, lax.rem(me, 2)
    grid = (n_ep, n_tp, me, me_tp)

    def order(index):
        return chip_order(index, half)

    normed = rms_scale(tokens[...], attn_gain[...])
    for index in range(n_ep):
        norm_send[index] = normed[:, index * depth : (index + 1) * depth].astype(BF16)
        token_send[index] = tokens[:, index * depth : (index + 1) * depth]
    pl.semaphore_wait(barrier, everyone - 1)

    sent = fan_out("ep", n_ep, me, lambda t: norm_send.at[t], norm_land, norm_ss, norm_rs, order)
    norm_land[order(me)] = norm_send[me]
    normed_wide = normed.astype(BF16).astype(F32)
    for head in range(heads):
        logit = forget_bias[0, head] + jnp.sum(
            normed_wide * forget_rows[head : head + 1, :].astype(F32), axis=-1, keepdims=True
        )
        forget_log = jnp.minimum(logit, 0.0) - jnp.log1p(jnp.exp(-jnp.abs(logit)))
        forget_logs[:, head, :] = jnp.broadcast_to(forget_log, (rows, size))
    collect("ep", n_ep, me, norm_land, norm_ss, norm_rs, order)
    joined = norm_land[...].reshape(n_ep * rows, depth)
    for index, weight in enumerate((query_weight_held, key_weight_held, value_weight_held)):
        loads[index].wait()
        part_send[:, :, :, index * hidden : (index + 1) * hidden] = dot32(
            joined, weight[...]
        ).reshape(2, half, rows, hidden)
    swap = pair_copy("ep", me, part_send.at[1 - core], part_land, part_ss, part_rs, 0)
    swap.start()
    swap.wait_recv()
    score_send[...] = part_send[core, :, :, : 2 * hidden] + part_land[:, :, : 2 * hidden]
    sent += chip_fan("ep", half, me, score_send, score_land, score_ss, score_rs)
    value_send[...] = (part_send[core, :, :, 2 * hidden :] + part_land[:, :, 2 * hidden :]).astype(
        BF16
    )
    sent += chip_fan("ep", half, me, value_send, value_land, value_ss, value_rs)
    sent.append(swap)
    sent += fan_out("ep", n_ep, me, lambda t: token_send.at[t], token_land, token_ss, token_rs)
    token_land[me] = token_send[me]
    chip_collect("ep", half, me, score_land, score_ss, score_rs)
    summed = total_of(score_land, half).astype(BF16).astype(F32)
    for head in range(heads):
        query_rows[:, head, :] = summed[:, head * size : (head + 1) * size]
        key_rows[:, head, :] = summed[:, hidden + head * size : hidden + (head + 1) * size]

    scale = 1.0 / math.sqrt(size)
    loads[3].wait()
    loads[4].wait()

    def score_step(seq, carry):
        for head in range(heads):
            query = query_rows[seq, head : head + 1, :].astype(BF16)
            scores[seq, head : head + 1, :] = lax.dot_general(
                query,
                keys_held[seq, head],
                (((1,), (1,)), ((), ())),
                preferred_element_type=F32,
            )
        return carry

    lax.fori_loop(0, rows, score_step, 0, unroll=4)
    positions = lax.broadcasted_iota(jnp.int32, (rows, heads, span), 2)
    sequences = lax.broadcasted_iota(jnp.int32, (rows, heads, size), 0)
    live_wide = jnp.zeros((rows, heads, size), jnp.int32)
    for seq in range(rows):
        live_wide = jnp.where(sequences == seq, lengths[0, seq], live_wide)
    lives = live_wide[:, :, 0:1]
    gate_all = gates[...]
    last_gate = jnp.sum(jnp.where(positions == lives - 1, gate_all, 0.0), axis=-1, keepdims=True)
    gate_now = last_gate + forget_logs[:, :, 0:1]
    score_all = scores[...] * scale + gate_now - gate_all
    score_all = jnp.where(positions < lives, score_all, -jnp.inf)
    own_score = jnp.sum(query_rows[...] * key_rows[...], axis=-1, keepdims=True) * scale
    row_top = jnp.maximum(jnp.max(score_all, axis=-1, keepdims=True), own_score)
    raised = jnp.exp(score_all - row_top)
    own_raised = jnp.exp(own_score - row_top)
    totals = jnp.sum(raised, axis=-1, keepdims=True) + own_raised
    scores[...] = raised / totals
    own_prob = (own_raised / totals).astype(BF16).astype(F32)

    def value_step(seq, carry):
        for head in range(heads):
            weight = scores[seq, head : head + 1, :].astype(BF16)
            mixed[seq, head : head + 1, :] = dot32(weight, values_held[seq, head])
        return carry

    lax.fori_loop(0, rows, value_step, 0, unroll=4)
    chip_collect("ep", half, me, value_land, value_ss, value_rs)
    value_sum = total_of(value_land, half).astype(BF16).astype(F32)
    for head in range(heads):
        value_rows[:, head, :] = value_sum[:, head * size : (head + 1) * size]
    mixed[...] = mixed[...] + own_prob * value_rows[...]
    for head in range(heads):
        attended[:, head * size : (head + 1) * size] = mixed[:, head, :].astype(BF16)

    sent += fan_out("ep", n_ep, me, lambda t: attended, att_land, att_ss, att_rs)
    att_land[me] = attended[...]
    collect("ep", n_ep, me, att_land, att_ss, att_rs)
    loads[5].wait()
    shares = dot32(att_land[...].reshape(n_ep * rows, hidden), output_weight_held[...])
    head_send[...] = shares.reshape(n_tp, group_rows, depth)
    sent += fan_out("tp", n_tp, me_tp, lambda t: head_send.at[t], head_land, head_ss, head_rs)
    head_land[me_tp] = head_send[me_tp]
    collect("tp", n_tp, me_tp, head_land, head_ss, head_rs)
    mix_send[...] = total_of(head_land, n_tp).reshape(ratio, rows, depth)
    spread_rows("ep", "tp", *grid, mix_send, mix_land, mix_ss, mix_rs)
    sent += fan_out("tp", n_tp, me_tp, lambda t: mix_send, share_land, share_ss, share_rs)
    share_land[me_tp] = mix_send[...]
    collect("ep", n_ep, me, token_land, token_ss, token_rs)
    collect("tp", n_tp, me_tp, share_land, share_ss, share_rs)

    shared = share_land[...].reshape(n_ep, rows, depth)
    residual_part = (token_land[...].astype(F32) + shared).astype(BF16)
    dense_rows = (residual_part.astype(F32) * gain_parts[me]).astype(BF16)
    dense_rows = dense_rows.reshape(n_ep * rows, depth)
    for index, weight in enumerate((dense_gate_held, dense_up_held)):
        loads[6 + index].wait()
        product = dot32(dense_rows, weight[...])
        for place in range(n_ep):
            pair_send[place % 2, place // 2, :, index * hidden : (index + 1) * hidden] = product[
                place * rows : (place + 1) * rows
            ]
    swap = pair_copy("ep", me, pair_send.at[1 - core], pair_land, pair_ss, pair_rs, 0)
    swap.start()
    swap.wait_recv()
    sent.append(swap)
    dense_send[...] = (pair_send[core] + pair_land[...]).astype(BF16)
    sent += chip_fan("ep", half, me, dense_send, dense_land, dense_ss, dense_rs)

    spread_wait("ep", "tp", *grid, mix_send, mix_land, mix_ss, mix_rs)
    for index in range(n_ep):
        full[:, index * depth : (index + 1) * depth] = mix_land[index]
    residual = (tokens[...].astype(F32) + full[...]).astype(BF16)
    residual_wide = residual.astype(F32)
    row_scale = lax.rsqrt(
        jnp.mean(residual_wide * residual_wide, axis=-1, keepdims=True) + EPSILON
    )
    ffn_in = (residual_wide * row_scale * gain[...]).astype(BF16)

    outbound = dot32(to_slots[...], ffn_in)
    for index in range(n_ep):
        slot_send[index] = outbound[index * slots : (index + 1) * slots].astype(BF16)
    sent += fan_out("ep", n_ep, me, lambda t: slot_send.at[t], slot_land, slot_ss, slot_rs)
    slot_land[me] = slot_send[me]
    mix = jax.nn.sigmoid(
        jnp.sum(ffn_in.astype(F32) * dense_mix[...].astype(F32), axis=-1, keepdims=True)
    )

    chip_collect("ep", half, me, dense_land, dense_ss, dense_rs)
    dense_sum = total_of(dense_land, half) * row_scale
    dense_first = dense_sum[:, :hidden]
    hidden_send[...] = (
        dense_first / (1.0 + jnp.exp(-dense_first)) * dense_sum[:, hidden:]
    ).astype(BF16)
    sent += fan_out("ep", n_ep, me, lambda t: hidden_send, hidden_land, hidden_ss, hidden_rs)
    hidden_land[me] = hidden_send[...]

    collect("ep", n_ep, me, slot_land, slot_ss, slot_rs)
    for load in loads[8:]:
        load.wait()
    slot_rows = jnp.concatenate(
        [slot_land[index].astype(F32) for index in range(n_ep)], axis=0
    ).astype(BF16)
    gate_part = dot32(slot_rows, expert_gate_held[0])
    up_part = dot32(slot_rows, expert_up_held[0])
    expert_hidden = (gate_part / (1.0 + jnp.exp(-gate_part)) * up_part).astype(BF16)
    chunk = model // n_tp
    for index in range(n_tp):
        expert_send[index] = dot32(
            expert_hidden, expert_down_held[0, :, index * chunk : (index + 1) * chunk]
        ).astype(BF16)
    sent += fan_out(
        "tp", n_tp, me_tp, lambda t: expert_send.at[t], expert_land, expert_ss, expert_rs
    )
    expert_land[me_tp] = expert_send[me_tp]

    collect("tp", n_tp, me_tp, expert_land, expert_ss, expert_rs)
    expert_total = total_of(expert_land, n_tp)
    for index in range(n_ep):
        back_send[index] = expert_total[index * slots : (index + 1) * slots].astype(BF16)
    sent += fan_out("ep", n_ep, me, lambda t: back_send.at[t], back_land, back_ss, back_rs)
    back_land[me] = back_send[me]

    collect("ep", n_ep, me, hidden_land, hidden_ss, hidden_rs)
    down = dot32(hidden_land[...].reshape(n_ep * rows, hidden), dense_down_held[...])
    down_send[...] = down.astype(BF16).reshape(n_tp, group_rows, depth)
    sent += fan_out("tp", n_tp, me_tp, lambda t: down_send.at[t], down_land, down_ss, down_rs)
    down_land[me_tp] = down_send[me_tp]

    collect("ep", n_ep, me, back_land, back_ss, back_rs)
    back_rows = jnp.concatenate(
        [back_land[index].astype(F32) for index in range(n_ep)], axis=0
    ).astype(BF16)
    route_send[...] = routes[:, 0:1] * dot32(from_first[...], back_rows) + routes[:, 1:2] * dot32(
        from_second[...], back_rows
    )
    sent += fan_out("tp", n_tp, me_tp, lambda t: route_send, route_land, route_ss, route_rs)
    route_land[me_tp] = route_send[...]

    collect("tp", n_tp, me_tp, down_land, down_ss, down_rs)
    tail_send[...] = total_of(down_land, n_tp).astype(BF16).reshape(ratio, rows, depth)
    spread_rows("ep", "tp", *grid, tail_send, tail_land, tail_ss, tail_rs)
    collect("tp", n_tp, me_tp, route_land, route_ss, route_rs)
    spread_wait("ep", "tp", *grid, tail_send, tail_land, tail_ss, tail_rs)
    for index in range(n_ep):
        full[:, index * depth : (index + 1) * depth] = tail_land[index].astype(F32)
    for index in range(n_tp):
        span = slice(index * chunk, (index + 1) * chunk)
        out[:, span] = (
            residual[:, span].astype(F32) + route_land[index] + mix * full[:, span]
        ).astype(BF16)
    for copy in sent:
        copy.wait_send()
    spread_sent("ep", "tp", *grid, mix_send, mix_land, mix_ss, mix_rs)
    spread_sent("ep", "tp", *grid, tail_send, tail_land, tail_ss, tail_rs)


def layer(n_ep, n_tp, slots, scalars, small, large):
    rows, model = small[0].shape
    depth, hidden = large[0].shape
    heads, span, size = large[3].shape[1:]
    group_rows = n_ep * rows // n_tp
    ratio = n_ep // n_tp
    half = n_ep // 2
    chunk = model // n_tp
    vmem = pl.BlockSpec(memory_space=pltpu.VMEM)
    smem = pl.BlockSpec(memory_space=pltpu.SMEM)
    hbm = pl.BlockSpec(memory_space=pltpu.HBM)
    return pl.pallas_call(
        functools.partial(layer_kernel, n_ep, n_tp),
        out_shape=jax.ShapeDtypeStruct((rows, model), BF16),
        in_specs=[smem] * 2 + [vmem] * len(small) + [hbm] * len(large),
        out_specs=vmem,
        scratch_shapes=[
            pltpu.VMEM(large[0].shape, BF16),
            pltpu.VMEM(large[1].shape, BF16),
            pltpu.VMEM(large[2].shape, BF16),
            pltpu.VMEM(large[3].shape, BF16),
            pltpu.VMEM(large[4].shape, BF16),
            pltpu.VMEM(large[5].shape, BF16),
            pltpu.VMEM(large[6].shape, BF16),
            pltpu.VMEM(large[7].shape, BF16),
            pltpu.VMEM(large[8].shape, BF16),
            pltpu.VMEM(large[9].shape, BF16),
            pltpu.VMEM(large[10].shape, BF16),
            pltpu.VMEM(large[11].shape, BF16),
            pltpu.SemaphoreType.DMA((12,)),
            pltpu.VMEM((n_ep, rows, depth), BF16),
            pltpu.VMEM((n_ep, rows, depth), BF16),
            pltpu.SemaphoreType.DMA((n_ep,)),
            pltpu.SemaphoreType.DMA((n_ep,)),
            pltpu.VMEM((2, half, rows, 3 * hidden), F32),
            pltpu.VMEM((half, rows, 3 * hidden), F32),
            pltpu.SemaphoreType.DMA((1,)),
            pltpu.SemaphoreType.DMA((1,)),
            pltpu.VMEM((half, rows, 2 * hidden), F32),
            pltpu.VMEM((half, rows, 2 * hidden), F32),
            pltpu.SemaphoreType.DMA((half,)),
            pltpu.SemaphoreType.DMA((half,)),
            pltpu.VMEM((half, rows, hidden), BF16),
            pltpu.VMEM((half, rows, hidden), BF16),
            pltpu.SemaphoreType.DMA((half,)),
            pltpu.SemaphoreType.DMA((half,)),
            pltpu.VMEM((rows, heads, size), F32),
            pltpu.VMEM((rows, heads, size), F32),
            pltpu.VMEM((rows, heads, size), F32),
            pltpu.VMEM((rows, heads, size), F32),
            pltpu.VMEM((rows, heads, span), F32),
            pltpu.VMEM((rows, heads, size), F32),
            pltpu.VMEM((rows, hidden), BF16),
            pltpu.VMEM((rows, model), F32),
            pltpu.VMEM((n_ep, rows, hidden), BF16),
            pltpu.SemaphoreType.DMA((n_ep,)),
            pltpu.SemaphoreType.DMA((n_ep,)),
            pltpu.VMEM((n_tp, group_rows, depth), F32),
            pltpu.VMEM((n_tp, group_rows, depth), F32),
            pltpu.SemaphoreType.DMA((n_tp,)),
            pltpu.SemaphoreType.DMA((n_tp,)),
            pltpu.VMEM((ratio, rows, depth), F32),
            pltpu.VMEM((n_ep, rows, depth), F32),
            pltpu.SemaphoreType.DMA((n_ep,)),
            pltpu.SemaphoreType.DMA((n_ep,)),
            pltpu.VMEM((n_ep, rows, depth), BF16),
            pltpu.VMEM((n_ep, rows, depth), BF16),
            pltpu.SemaphoreType.DMA((n_ep,)),
            pltpu.SemaphoreType.DMA((n_ep,)),
            pltpu.VMEM((n_tp, ratio, rows, depth), F32),
            pltpu.SemaphoreType.DMA((n_tp,)),
            pltpu.SemaphoreType.DMA((n_tp,)),
            pltpu.VMEM((n_ep, slots, model), BF16),
            pltpu.VMEM((n_ep, slots, model), BF16),
            pltpu.SemaphoreType.DMA((n_ep,)),
            pltpu.SemaphoreType.DMA((n_ep,)),
            pltpu.VMEM((2, half, rows, 2 * hidden), F32),
            pltpu.VMEM((half, rows, 2 * hidden), F32),
            pltpu.SemaphoreType.DMA((1,)),
            pltpu.SemaphoreType.DMA((1,)),
            pltpu.VMEM((half, rows, 2 * hidden), BF16),
            pltpu.VMEM((half, rows, 2 * hidden), BF16),
            pltpu.SemaphoreType.DMA((half,)),
            pltpu.SemaphoreType.DMA((half,)),
            pltpu.VMEM((n_tp, n_ep * slots, chunk), BF16),
            pltpu.VMEM((n_tp, n_ep * slots, chunk), BF16),
            pltpu.SemaphoreType.DMA((n_tp,)),
            pltpu.SemaphoreType.DMA((n_tp,)),
            pltpu.VMEM((n_ep, slots, chunk), BF16),
            pltpu.VMEM((n_ep, slots, chunk), BF16),
            pltpu.SemaphoreType.DMA((n_ep,)),
            pltpu.SemaphoreType.DMA((n_ep,)),
            pltpu.VMEM((rows, hidden), BF16),
            pltpu.VMEM((n_ep, rows, hidden), BF16),
            pltpu.SemaphoreType.DMA((n_ep,)),
            pltpu.SemaphoreType.DMA((n_ep,)),
            pltpu.VMEM((n_tp, group_rows, depth), BF16),
            pltpu.VMEM((n_tp, group_rows, depth), BF16),
            pltpu.SemaphoreType.DMA((n_tp,)),
            pltpu.SemaphoreType.DMA((n_tp,)),
            pltpu.VMEM((ratio, rows, depth), BF16),
            pltpu.VMEM((n_ep, rows, depth), BF16),
            pltpu.SemaphoreType.DMA((n_ep,)),
            pltpu.SemaphoreType.DMA((n_ep,)),
            pltpu.VMEM((rows, chunk), F32),
            pltpu.VMEM((n_tp, rows, chunk), F32),
            pltpu.SemaphoreType.DMA((n_tp,)),
            pltpu.SemaphoreType.DMA((n_tp,)),
        ],
        compiler_params=pltpu.CompilerParams(
            collective_id=0, has_side_effects=True, vmem_limit_bytes=60 * 1024 * 1024
        ),
    )(*scalars, *small, *large)


def shards(
    tokens,
    attn_gain,
    query_weight,
    key_weight,
    value_weight,
    forget_weight,
    forget_bias,
    cache_keys,
    cache_values,
    cache_gates,
    lengths,
    output_weight,
    ffn_gain,
    dense_gate_proj,
    dense_up_proj,
    dense_down_proj,
    dense_mix,
    expert_ids,
    group_prob,
    pair_prob,
    expert_gate,
    expert_up,
    expert_down,
):
    seq_count = tokens.shape[0]
    n_ep = lax.axis_size("ep")
    n_tp = lax.axis_size("tp")
    expert_count = n_ep * expert_gate.shape[0]
    capacity = max(4 * seq_count // expert_count, 8)
    slot_total = expert_count * capacity
    picks = expert_ids.reshape(-1)
    same = (picks[:, None] == picks[None, :]).astype(jnp.int32)
    before = jnp.tril(jnp.ones((2 * seq_count, 2 * seq_count), jnp.int32), -1)
    slot_rank = jnp.sum(same * before, axis=1)
    destination = (picks * capacity + slot_rank).reshape(seq_count, 2)
    slot_grid = jnp.arange(slot_total, dtype=jnp.int32)
    select_first = (destination[:, 0:1] == slot_grid[None, :]).astype(jnp.bfloat16)
    select_second = (destination[:, 1:2] == slot_grid[None, :]).astype(jnp.bfloat16)
    to_slots = (select_first + select_second).T
    routes = group_prob[:, None] * pair_prob / jnp.sum(pair_prob, axis=1, keepdims=True)
    model = (1, tokens.shape[1])
    return layer(
        n_ep,
        n_tp,
        capacity,
        (forget_bias.reshape(1, -1), lengths.reshape(1, -1)),
        (
            tokens,
            attn_gain.reshape(model),
            forget_weight.T,
            cache_gates,
            ffn_gain.reshape(model),
            ffn_gain.reshape(n_ep, 1, -1),
            dense_mix.reshape(model),
            to_slots,
            select_first,
            select_second,
            routes,
        ),
        (
            query_weight,
            key_weight,
            value_weight,
            cache_keys,
            cache_values,
            output_weight,
            dense_gate_proj,
            dense_up_proj,
            expert_gate,
            expert_up,
            expert_down,
            dense_down_proj,
        ),
    )


def solution(mesh):
    return jax.shard_map(
        shards,
        mesh=mesh,
        in_specs=(
            P("ep", None),
            P(),
            P("ep", "tp"),
            P("ep", "tp"),
            P("ep", "tp"),
            P(None, "tp"),
            P("tp"),
            P("ep", "tp", None, None),
            P("ep", "tp", None, None),
            P("ep", "tp", None),
            P("ep"),
            P("tp", "ep"),
            P(),
            P("ep", "tp"),
            P("ep", "tp"),
            P("tp", "ep"),
            P(),
            P("ep", None),
            P("ep"),
            P("ep", None),
            P("ep", None, "tp"),
            P("ep", None, "tp"),
            P("ep", "tp", None),
        ),
        out_specs=P("ep", None),
        check_vma=False,
    )
```

profile of v0, /device:TPU:0, one launch (start us, length us, event | category | flops | bytes accessed | tf_op | source)
XLA Modules:
  0.0 79.3 jit_solution(41530277424294660)
XLA Ops:
  0.0 0.7 fusion.5
  0.7 0.1 copy.41
  0.8 0.7 broadcast_divide_fusion.routes
  1.5 1.3 %reshape.30.dense_mix = bf16[1,2048]{1,0:T(2,128)(2,1)} reshape(bf16[2048]{0:T(1024)(128)(2,1)} %param.39) | data formatting | bytes 8192 | tf_op jit(solution)/shard_map/reshape | solution.py:731
  2.7 0.8 copy.39
  3.5 0.1 eq.59
  3.6 0.2 select_reduce_fusion
  3.8 0.1 reduce_sum.21
  3.9 0.1 copy.40
  3.9 0.7 multiply_add_fusion
  4.7 0.7 fusion.3
  5.3 0.6 fusion.2.to_slots
  5.9 71.9 %shard_map.217 = bf16[16,2048]{1,0:T(8,128)(2,1)} custom-call(f32[1,4]{1,0:T(1,128)} %bitcast.14, s32[1,16]{1,0:T(1,128)} %bitcast.15, bf16[16,2048]{1,0:T(8,128)(2,1)} %tokens.1, f32[1,2048]{1,0:T(1,128)} %bitcast.13, bf16[4,2048]{1,0:T(4,128)(2,1)} %bitcast.12, f32[16,4,384]{2,1,0:T(4,128)} %gates.1, f32[1,2048]{1,0:T(1,128)} %bitcast.10, ...), custom_call_target="tpu_custom_call" | custom-call | tf_op jit(solution)/shard_map/pallas_call | solution.py:573
  77.8 1.5 %copy.44 = bf16[16,2048]{1,0:T(8,128)(2,1)} copy(bf16[16,2048]{1,0:T(8,128)(2,1)} %shard_map.217) | data formatting | bytes 131072
  (2 shorter events, 0.0 us)
where the time goes:
time: 79.6 us; the launch traced here: 79.3 us
  Pallas kernels  71.9 us (90%)
  local copies, waits for them, and re-layouts  3.86 us (5%)
  other arithmetic  3.54 us (4%)
    pallas_call x1, Pallas kernels, layer(): pl.pallas_call(functools.partial(layer_kernel, n_ep, n_tp), out_shape=jax...  71.9 us
    unnamed x2, local copies, waits for them, and re-layouts  2.23 us

commit v1 on v0

--- a/solution.py
+++ b/solution.py
@@ -188,6 +188,46 @@
         ).wait_recv()
 
 
+def pick(one_hot, held):
+    return lax.dot_general(
+        one_hot, held, (((0,), (0,)), ((), ())), preferred_element_type=F32
+    )
+
+
+def slot_tables(expert_ids, group_prob, pair_prob, experts, slots):
+    rows = expert_ids.shape[1]
+    ids = expert_ids[...]
+    row_at = lax.broadcasted_iota(jnp.int32, (rows, rows), 0)
+    row_to = lax.broadcasted_iota(jnp.int32, (rows, rows), 1)
+    expert_at = lax.broadcasted_iota(jnp.int32, (experts, rows), 0)
+    first = ids[0:1, :] == expert_at
+    second = ids[1:2, :] == expert_at
+    hits = (first | second).astype(F32).astype(BF16)
+    earlier = (row_at < row_to).astype(F32).astype(BF16)
+    ranks = dot32(hits, earlier)
+    slot_at = lax.broadcasted_iota(jnp.int32, (slots, rows), 0).astype(F32)
+    tables = []
+    for chosen in (first, second):
+        place = jnp.where(chosen, ranks, -1.0)
+        tables.append(
+            jnp.concatenate(
+                [
+                    (place[expert : expert + 1, :] == slot_at).astype(F32)
+                    for expert in range(experts)
+                ],
+                axis=0,
+            )
+        )
+    probs = pair_prob[...]
+    shares = group_prob[...] * probs / (probs[0:1, :] + probs[1:2, :])
+    columns = [
+        jnp.sum(jnp.where(row_at == row_to, shares[k : k + 1, :], 0.0), axis=-1, keepdims=True)
+        for k in range(2)
+    ]
+    both = (tables[0] + tables[1]).astype(BF16)
+    return tables[0].astype(BF16), tables[1].astype(BF16), both, columns[0], columns[1]
+
+
 def layer_kernel(
     n_ep,
     n_tp,
@@ -200,10 +240,9 @@
     gain,
     gain_parts,
     dense_mix,
-    to_slots,
-    from_first,
-    from_second,
-    routes,
+    expert_ids,
+    group_prob,
+    pair_prob,
     query_weight,
     key_weight,
     value_weight,
@@ -355,6 +394,8 @@
 
     sent = fan_out("ep", n_ep, me, lambda t: norm_send.at[t], norm_land, norm_ss, norm_rs, order)
     norm_land[order(me)] = norm_send[me]
+    sent += fan_out("ep", n_ep, me, lambda t: token_send.at[t], token_land, token_ss, token_rs)
+    token_land[me] = token_send[me]
     normed_wide = normed.astype(BF16).astype(F32)
     for head in range(heads):
         logit = forget_bias[0, head] + jnp.sum(
@@ -364,28 +405,38 @@
         forget_logs[:, head, :] = jnp.broadcast_to(forget_log, (rows, size))
     collect("ep", n_ep, me, norm_land, norm_ss, norm_rs, order)
     joined = norm_land[...].reshape(n_ep * rows, depth)
+    swaps = []
     for index, weight in enumerate((query_weight_held, key_weight_held, value_weight_held)):
         loads[index].wait()
-        part_send[:, :, :, index * hidden : (index + 1) * hidden] = dot32(
-            joined, weight[...]
-        ).reshape(2, half, rows, hidden)
-    swap = pair_copy("ep", me, part_send.at[1 - core], part_land, part_ss, part_rs, 0)
-    swap.start()
-    swap.wait_recv()
-    score_send[...] = part_send[core, :, :, : 2 * hidden] + part_land[:, :, : 2 * hidden]
-    sent += chip_fan("ep", half, me, score_send, score_land, score_ss, score_rs)
-    value_send[...] = (part_send[core, :, :, 2 * hidden :] + part_land[:, :, 2 * hidden :]).astype(
-        BF16
+        part_send[index] = dot32(joined, weight[...]).reshape(2, half, rows, hidden)
+        swap = pair_copy(
+            "ep", me, part_send.at[index, 1 - core], part_land.at[index], part_ss, part_rs, index
+        )
+        swap.start()
+        swaps.append(swap)
+    sent += swaps
+    for index in range(2):
+        swaps[index].wait_recv()
+        score_send[index] = part_send[index, core] + part_land[index]
+        sent += chip_fan(
+            "ep",
+            half,
+            me,
+            score_send.at[index],
+            score_land.at[index],
+            score_ss.at[index],
+            score_rs.at[index],
+        )
+    swaps[2].wait_recv()
+    value_send[...] = (part_send[2, core] + part_land[2]).astype(BF16)
+    sent += chip_fan("ep", half, me, value_send, value_land, value_ss, value_rs)
+    to_first, to_second, to_slots, first_route, second_route = slot_tables(
+        expert_ids, group_prob, pair_prob, n_ep, slots
     )
-    sent += chip_fan("ep", half, me, value_send, value_land, value_ss, value_rs)
-    sent.append(swap)
-    sent += fan_out("ep", n_ep, me, lambda t: token_send.at[t], token_land, token_ss, token_rs)
-    token_land[me] = token_send[me]
-    chip_collect("ep", half, me, score_land, score_ss, score_rs)
-    summed = total_of(score_land, half).astype(BF16).astype(F32)
+    chip_collect("ep", half, me, score_land.at[0], score_ss.at[0], score_rs.at[0])
+    summed = total_of(score_land.at[0], half).astype(BF16).astype(F32)
     for head in range(heads):
         query_rows[:, head, :] = summed[:, head * size : (head + 1) * size]
-        key_rows[:, head, :] = summed[:, hidden + head * size : hidden + (head + 1) * size]
 
     scale = 1.0 / math.sqrt(size)
     loads[3].wait()
@@ -403,6 +454,10 @@
         return carry
 
     lax.fori_loop(0, rows, score_step, 0, unroll=4)
+    chip_collect("ep", half, me, score_land.at[1], score_ss.at[1], score_rs.at[1])
+    summed = total_of(score_land.at[1], half).astype(BF16).astype(F32)
+    for head in range(heads):
+        key_rows[:, head, :] = summed[:, head * size : (head + 1) * size]
     positions = lax.broadcasted_iota(jnp.int32, (rows, heads, span), 2)
     sequences = lax.broadcasted_iota(jnp.int32, (rows, heads, size), 0)
     live_wide = jnp.zeros((rows, heads, size), jnp.int32)
@@ -481,14 +536,18 @@
     )
     ffn_in = (residual_wide * row_scale * gain[...]).astype(BF16)
 
-    outbound = dot32(to_slots[...], ffn_in)
+    outbound = dot32(to_slots, ffn_in)
     for index in range(n_ep):
         slot_send[index] = outbound[index * slots : (index + 1) * slots].astype(BF16)
     sent += fan_out("ep", n_ep, me, lambda t: slot_send.at[t], slot_land, slot_ss, slot_rs)
     slot_land[me] = slot_send[me]
-    mix = jax.nn.sigmoid(
-        jnp.sum(ffn_in.astype(F32) * dense_mix[...].astype(F32), axis=-1, keepdims=True)
-    )
+    lanes = dense_mix.shape[1]
+    mix_sum = jnp.zeros((rows, lanes), F32)
+    for index in range(model // lanes):
+        mix_sum = mix_sum + ffn_in[:, index * lanes : (index + 1) * lanes].astype(F32) * dense_mix[
+            index : index + 1, :
+        ].astype(F32)
+    mix = jax.nn.sigmoid(jnp.sum(mix_sum, axis=-1, keepdims=True))
 
     chip_collect("ep", half, me, dense_land, dense_ss, dense_rs)
     dense_sum = total_of(dense_land, half) * row_scale
@@ -535,8 +594,8 @@
     back_rows = jnp.concatenate(
         [back_land[index].astype(F32) for index in range(n_ep)], axis=0
     ).astype(BF16)
-    route_send[...] = routes[:, 0:1] * dot32(from_first[...], back_rows) + routes[:, 1:2] * dot32(
-        from_second[...], back_rows
+    route_send[...] = first_route * pick(to_first, back_rows) + second_route * pick(
+        to_second, back_rows
     )
     sent += fan_out("tp", n_tp, me_tp, lambda t: route_send, route_land, route_ss, route_rs)
     route_land[me_tp] = route_send[...]
@@ -593,14 +652,14 @@
             pltpu.VMEM((n_ep, rows, depth), BF16),
             pltpu.SemaphoreType.DMA((n_ep,)),
             pltpu.SemaphoreType.DMA((n_ep,)),
-            pltpu.VMEM((2, half, rows, 3 * hidden), F32),
-            pltpu.VMEM((half, rows, 3 * hidden), F32),
-            pltpu.SemaphoreType.DMA((1,)),
-            pltpu.SemaphoreType.DMA((1,)),
-            pltpu.VMEM((half, rows, 2 * hidden), F32),
-            pltpu.VMEM((half, rows, 2 * hidden), F32),
-            pltpu.SemaphoreType.DMA((half,)),
-            pltpu.SemaphoreType.DMA((half,)),
+            pltpu.VMEM((3, 2, half, rows, hidden), F32),
+            pltpu.VMEM((3, half, rows, hidden), F32),
+            pltpu.SemaphoreType.DMA((3,)),
+            pltpu.SemaphoreType.DMA((3,)),
+            pltpu.VMEM((2, half, rows, hidden), F32),
+            pltpu.VMEM((2, half, rows, hidden), F32),
+            pltpu.SemaphoreType.DMA((2, half)),
+            pltpu.SemaphoreType.DMA((2, half)),
             pltpu.VMEM((half, rows, hidden), BF16),
             pltpu.VMEM((half, rows, hidden), BF16),
             pltpu.SemaphoreType.DMA((half,)),
@@ -704,17 +763,6 @@
     n_tp = lax.axis_size("tp")
     expert_count = n_ep * expert_gate.shape[0]
     capacity = max(4 * seq_count // expert_count, 8)
-    slot_total = expert_count * capacity
-    picks = expert_ids.reshape(-1)
-    same = (picks[:, None] == picks[None, :]).astype(jnp.int32)
-    before = jnp.tril(jnp.ones((2 * seq_count, 2 * seq_count), jnp.int32), -1)
-    slot_rank = jnp.sum(same * before, axis=1)
-    destination = (picks * capacity + slot_rank).reshape(seq_count, 2)
-    slot_grid = jnp.arange(slot_total, dtype=jnp.int32)
-    select_first = (destination[:, 0:1] == slot_grid[None, :]).astype(jnp.bfloat16)
-    select_second = (destination[:, 1:2] == slot_grid[None, :]).astype(jnp.bfloat16)
-    to_slots = (select_first + select_second).T
-    routes = group_prob[:, None] * pair_prob / jnp.sum(pair_prob, axis=1, keepdims=True)
     model = (1, tokens.shape[1])
     return layer(
         n_ep,
@@ -728,11 +776,10 @@
             cache_gates,
             ffn_gain.reshape(model),
             ffn_gain.reshape(n_ep, 1, -1),
-            dense_mix.reshape(model),
-            to_slots,
-            select_first,
-            select_second,
-            routes,
+            dense_mix.reshape(-1, 128),
+            expert_ids.T,
+            group_prob.reshape(1, -1),
+            pair_prob.T,
         ),
         (
             query_weight,

time: 79.6 us -> 71.4 us (0.90)
  other arithmetic: 3.54 us -> 0 us
  local copies, waits for them, and re-layouts: 3.86 us -> 1.47 us
  Pallas kernels: 71.9 us -> 69.6 us
    pallas_call x1, Pallas kernels: 71.9 us -> 69.6 us  [layer(): pl.pallas_call(functools.partial(layer_kernel, n_ep, n_tp), out_shape=jax...]
    add x3 -> x0, other arithmetic: 1.32 us -> none  [the longest x1 0.7 us: shards(): destination = (picks * capacity + slot_rank).reshape(seq_count, 2)]
    reshape x1 -> x0, local copies, waits for them, and re-layouts: 1.28 us -> none  [shards(): dense_mix.reshape(model)]
    reduce_sum x2 -> x0, other arithmetic: 0.88 us -> none  [the longest x1 0.7 us: shards(): jnp.sum(pair_prob, axis=1, keepdims=True)]
    unnamed x2 -> x1, local copies, waits for them, and re-layouts: 2.23 us -> 1.47 us
where the time goes in v1:
time: 71.4 us; the launch traced here: 71.1 us
  Pallas kernels  69.6 us (97%)
  local copies, waits for them, and re-layouts  1.47 us (2%)
    pallas_call x1, Pallas kernels, layer(): pl.pallas_call(functools.partial(layer_kernel, n_ep, n_tp), out_shape=jax...  69.6 us
    unnamed x1, local copies, waits for them, and re-layouts  1.47 us

profile of v1, /device:TPU:0, one launch (start us, length us, event | category | flops | bytes accessed | tf_op | source)
XLA Modules:
  0.0 71.1 jit_solution(16068725111789730092)
XLA Ops:
  0.0 69.6 %shard_map.217 = bf16[16,2048]{1,0:T(8,128)(2,1)} custom-call(f32[1,4]{1,0:T(1,128)} %bitcast.17, s32[1,16]{1,0:T(1,128)} %bitcast.18, bf16[16,2048]{1,0:T(8,128)(2,1)} %tokens.1, f32[1,2048]{1,0:T(1,128)} %bitcast.13, bf16[4,2048]{1,0:T(4,128)(2,1)} %bitcast.12, f32[16,4,384]{2,1,0:T(4,128)} %gates.1, f32[1,2048]{1,0:T(1,128)} %bitcast.10, ...), custom_call_target="tpu_custom_call" | custom-call | tf_op jit(solution)/shard_map/pallas_call | solution.py:632
  69.7 1.5 %copy.25 = bf16[16,2048]{1,0:T(8,128)(2,1)} copy(bf16[16,2048]{1,0:T(8,128)(2,1)} %shard_map.217) | data formatting | bytes 131072

commit v2 on v1

v2 whole, which is shorter than its diff:
```python
import functools
import math

import jax
import jax.numpy as jnp
from jax import lax
from jax.experimental import pallas as pl
from jax.experimental.pallas import tpu as pltpu
from jax.sharding import PartitionSpec as P

EPSILON = 1e-06


def rms_scale(values, norm_gain):
    widened = values.astype(jnp.float32)
    return (
        widened
        * lax.rsqrt(jnp.mean(widened * widened, axis=-1, keepdims=True) + EPSILON)
        * norm_gain
    )


MESH = pl.DeviceIdType.MESH
F32 = jnp.float32
BF16 = jnp.bfloat16


def flip(me, step):
    bit = 1
    while bit <= step:
        if step & bit:
            me = me + bit - 2 * bit * lax.rem(me // bit, 2)
        bit *= 2
    return me


def toward(me, step, count):
    return flip(me, step) if count & (count - 1) == 0 else lax.rem(me + step, count)


def origin(me, step, count):
    return flip(me, step) if count & (count - 1) == 0 else lax.rem(me + count - step, count)


def far_first(count):
    return range(count - 1, 0, -1)


def remote(source, place, send_sem, recv_sem, device):
    return pltpu.make_async_remote_copy(
        src_ref=source,
        dst_ref=place,
        send_sem=send_sem,
        recv_sem=recv_sem,
        device_id=device,
        device_id_type=MESH,
    )


def fan_out(axis, count, me, source_of, landing, send_sem, recv_sem, slot=None):
    copies = []
    place = me if slot is None else slot(me)
    for step in far_first(count):
        target = toward(me, step, count)
        copy = remote(
            source_of(target),
            landing.at[place],
            send_sem.at[step],
            recv_sem.at[me],
            {axis: target},
        )
        copy.start()
        copies.append(copy)
    return copies


def arrive(axis, source, place, send_sem, recv_sem):
    remote(place, place, send_sem, recv_sem, {axis: source}).wait_recv()


def collect(axis, count, me, landing, send_sem, recv_sem, slot=None):
    for step in range(1, count):
        source = origin(me, step, count)
        place = source if slot is None else slot(source)
        arrive(axis, source, landing.at[place], send_sem.at[step], recv_sem.at[source])


def total_of(ref, count):
    total = ref[0].astype(F32)
    for index in range(1, count):
        total = total + ref[index].astype(F32)
    return total


def dot32(left, right):
    return jnp.dot(left, right, preferred_element_type=F32)


def silu(values):
    return values / (1.0 + jnp.exp(-values))


def chip_order(index, half):
    return lax.rem(index, 2) * half + index // 2


def pair_copy(axis, me, source, landing, send_sem, recv_sem, slot):
    return remote(
        source,
        landing,
        send_sem.at[slot],
        recv_sem.at[slot],
        {axis: me + 1 - 2 * lax.rem(me, 2)},
    )


def chip_fan(axis, half, me, held, landing, send_sem, recv_sem):
    chip, core = me // 2, lax.rem(me, 2)
    copies = []
    for step in far_first(half):
        target = toward(chip, step, half)
        copy = remote(
            held.at[target],
            landing.at[chip],
            send_sem.at[step],
            recv_sem.at[chip],
            {axis: target * 2 + core},
        )
        copy.start()
        copies.append(copy)
    landing[chip] = held[chip]
    return copies


def chip_collect(axis, half, me, landing, send_sem, recv_sem):
    chip, core = me // 2, lax.rem(me, 2)
    for step in range(1, half):
        source = origin(chip, step, half)
        arrive(
            axis, source * 2 + core, landing.at[source], send_sem.at[step], recv_sem.at[source]
        )


def pick(one_hot, held):
    return lax.dot_general(
        one_hot, held, (((0,), (0,)), ((), ())), preferred_element_type=F32
    )


def slot_tables(ids, experts, slots):
    rows = ids.shape[1]
    row_at = lax.broadcasted_iota(jnp.int32, (rows, rows), 0)
    row_to = lax.broadcasted_iota(jnp.int32, (rows, rows), 1)
    expert_at = lax.broadcasted_iota(jnp.int32, (experts, rows), 0).astype(F32)
    slot_at = lax.broadcasted_iota(jnp.int32, (slots, rows), 0).astype(F32)
    first = ids[0:1, :] == expert_at
    second = ids[1:2, :] == expert_at
    hits = (first | second).astype(F32).astype(BF16)
    earlier = (row_at < row_to).astype(F32).astype(BF16)
    ranks = dot32(hits, earlier)
    tables = []
    for chosen in (first, second):
        place = jnp.where(chosen, ranks, -1.0)
        tables.append(
            jnp.concatenate(
                [
                    (place[expert : expert + 1, :] == slot_at).astype(F32)
                    for expert in range(experts)
                ],
                axis=0,
            )
        )
    return tables


def route_columns(group_prob, pair_prob):
    rows = pair_prob.shape[1]
    row_at = lax.broadcasted_iota(jnp.int32, (rows, rows), 0)
    row_to = lax.broadcasted_iota(jnp.int32, (rows, rows), 1)
    probs = pair_prob[...]
    shares = group_prob[...] * probs / (probs[0:1, :] + probs[1:2, :])
    return [
        jnp.sum(jnp.where(row_at == row_to, shares[k : k + 1, :], 0.0), axis=-1, keepdims=True)
        for k in range(2)
    ]


def layer_kernel(
    n_ep,
    n_tp,
    forget_bias,
    lengths,
    tokens,
    attn_gain,
    forget_rows,
    gates,
    gain,
    gain_parts,
    dense_mix,
    expert_ids,
    group_prob,
    pair_prob,
    query_weight,
    key_weight,
    value_weight,
    keys,
    values,
    output_weight,
    dense_gate,
    dense_up,
    expert_gate,
    expert_up,
    expert_down,
    dense_down,
    out,
    query_weight_held,
    key_weight_held,
    value_weight_held,
    keys_held,
    values_held,
    output_weight_held,
    dense_gate_held,
    dense_up_held,
    expert_gate_held,
    expert_up_held,
    expert_down_held,
    dense_down_held,
    load_sem,
    norm_send,
    norm_land,
    norm_ss,
    norm_rs,
    ids_send,
    ids_land,
    ids_ss,
    ids_rs,
    token_send,
    token_land,
    token_ss,
    token_rs,
    part_send,
    part_land,
    part_ss,
    part_rs,
    score_send,
    score_land,
    score_ss,
    score_rs,
    value_send,
    value_land,
    value_ss,
    value_rs,
    query_rows,
    key_rows,
    value_rows,
    forget_logs,
    scores,
    mixed,
    attended,
    att_land,
    att_ss,
    att_rs,
    head_send,
    head_land,
    head_ss,
    head_rs,
    res_land,
    res_send,
    res_ss,
    res_rs,
    own_land,
    own_ss,
    own_rs,
    slot_send,
    slot_land,
    slot_ss,
    slot_rs,
    pass_ss,
    pass_rs,
    ffn_rows,
    mix_parts,
    pair_send,
    pair_land,
    pair_ss,
    pair_rs,
    dense_send,
    dense_land,
    dense_ss,
    dense_rs,
    hidden_send,
    hidden_land,
    hidden_ss,
    hidden_rs,
    expert_send,
    expert_land,
    expert_ss,
    expert_rs,
    back_send,
    back_land,
    back_ss,
    back_rs,
    tail_send,
    tail_land,
    tail_ss,
    tail_rs,
    quarter_land,
    quarter_ss,
    quarter_rs,
    route_part,
    out_send,
    out_land,
    out_ss,
    out_rs,
):
    me = lax.axis_index("ep")
    me_tp = lax.axis_index("tp")
    barrier = pltpu.get_barrier_semaphore()
    ratio = n_ep // n_tp
    half = n_ep // 2
    chip, core = me // 2, lax.rem(me, 2)
    spreads = me // ratio == me_tp
    part_at = lax.rem(me, ratio)

    def greet(axis, mine, count):
        def signal(step, carry):
            pl.semaphore_signal(
                barrier,
                inc=1,
                device_id={axis: lax.rem(mine + step, count)},
                device_id_type=MESH,
            )
            return carry

        lax.fori_loop(1, count, signal, 0, unroll=count <= 8)

    greet("ep", me, n_ep)
    greet("tp", me_tp, n_tp)
    sources = [query_weight, key_weight, value_weight, keys, values, output_weight, dense_gate, dense_up, expert_gate, expert_up, dense_down]
    places = [query_weight_held, key_weight_held, value_weight_held, keys_held, values_held, output_weight_held, dense_gate_held, dense_up_held, expert_gate_held, expert_up_held, dense_down_held]
    rows, model = tokens.shape
    depth, hidden = query_weight.shape
    heads, span, size = keys.shape[1:]
    slots = slot_send.shape[2]
    chunk = model // n_tp
    wide = 2 * hidden
    for index in range(n_tp):
        sources.append(expert_down.at[0, :, pl.ds(index * chunk, chunk)])
        places.append(expert_down_held.at[index])
    loads = [
        pltpu.make_async_copy(source, place, load_sem.at[index])
        for index, (source, place) in enumerate(zip(sources, places))
    ]
    for load in loads:
        load.start()

    def order(index):
        return chip_order(index, half)

    normed = rms_scale(tokens[...], attn_gain[...])
    for index in range(n_ep):
        norm_send[index] = normed[:, index * depth : (index + 1) * depth].astype(BF16)
        token_send[index] = tokens[:, index * depth : (index + 1) * depth]
    ids = expert_ids[...].astype(F32)
    ids_send[0:2, 0:rows] = ids
    pl.semaphore_wait(barrier, n_ep + n_tp - 2)

    sent = fan_out("ep", n_ep, me, lambda t: norm_send.at[t], norm_land, norm_ss, norm_rs, order)
    norm_land[order(me)] = norm_send[me]

    def row_copies(source_of, landing, send_sem, recv_sem):
        return [
            remote(
                source_of(toward(me, step, n_ep)),
                landing.at[part_at],
                send_sem.at[step],
                recv_sem.at[part_at],
                {"ep": toward(me, step, n_ep)},
            )
            for step in far_first(n_ep)
        ]

    def row_arrivals(base, landing, send_sem, recv_sem):
        for part in range(ratio):
            source = base * ratio + part

            @pl.when(source != me)
            def _():
                arrive("ep", source, landing.at[part], send_sem.at[0], recv_sem.at[part])

    spread_early = row_copies(lambda t: token_send.at[t], token_land, token_ss, token_rs)
    spread_early += row_copies(lambda t: ids_send, ids_land, ids_ss, ids_rs)

    @pl.when(spreads)
    def _():
        for copy in spread_early:
            copy.start()
        token_land[part_at] = token_send[me]
        ids_land[part_at] = ids_send[...]

    normed_wide = normed.astype(BF16).astype(F32)
    for head in range(heads):
        logit = forget_bias[0, head] + jnp.sum(
            normed_wide * forget_rows[head : head + 1, :].astype(F32), axis=-1, keepdims=True
        )
        forget_log = jnp.minimum(logit, 0.0) - jnp.log1p(jnp.exp(-jnp.abs(logit)))
        forget_logs[:, head, :] = jnp.broadcast_to(forget_log, (rows, size))
    mix_lanes = dense_mix.shape[1]
    mix_wide = dense_mix[...].astype(F32)
    for index in range(n_ep):
        for start in range(0, depth, min(depth, mix_lanes)):
            at = index * depth + start
            line, lane = at // mix_lanes, at % mix_lanes
            width = min(depth, mix_lanes)
            mix_parts[index, :, start : start + width] = mix_wide[
                line : line + 1, lane : lane + width
            ]
    first_table, second_table = slot_tables(ids, n_ep, slots)
    to_first, to_second = first_table.astype(BF16), second_table.astype(BF16)
    first_route, second_route = route_columns(group_prob, pair_prob)

    collect("ep", n_ep, me, norm_land, norm_ss, norm_rs, order)
    joined = norm_land[...].reshape(n_ep * rows, depth)
    swaps = []
    for index, weight in enumerate((query_weight_held, key_weight_held, value_weight_held)):
        loads[index].wait()
        part_send[index] = dot32(joined, weight[...]).reshape(2, half, rows, hidden)
        swap = pair_copy(
            "ep", me, part_send.at[index, 1 - core], part_land.at[index], part_ss, part_rs, index
        )
        swap.start()
        swaps.append(swap)
    sent += swaps
    for index in range(2):
        swaps[index].wait_recv()
        score_send[index] = part_send[index, core] + part_land[index]
        sent += chip_fan(
            "ep",
            half,
            me,
            score_send.at[index],
            score_land.at[index],
            score_ss.at[index],
            score_rs.at[index],
        )
    swaps[2].wait_recv()
    value_send[...] = (part_send[2, core] + part_land[2]).astype(BF16)
    sent += chip_fan("ep", half, me, value_send, value_land, value_ss, value_rs)
    row_arrivals(me_tp, ids_land, ids_ss, ids_rs)
    dispatch = []
    for part in range(ratio):
        tables = slot_tables(ids_land[part][0:2, 0:rows], n_ep, slots)
        dispatch.append((tables[0] + tables[1]).astype(BF16))
    row_arrivals(me_tp, token_land, token_ss, token_rs)
    chip_collect("ep", half, me, score_land.at[0], score_ss.at[0], score_rs.at[0])
    summed = total_of(score_land.at[0], half).astype(BF16).astype(F32)
    for head in range(heads):
        query_rows[:, head, :] = summed[:, head * size : (head + 1) * size]

    scale = 1.0 / math.sqrt(size)
    loads[3].wait()
    loads[4].wait()

    def score_step(seq, carry):
        for head in range(heads):
            query = query_rows[seq, head : head + 1, :].astype(BF16)
            scores[seq, head : head + 1, :] = lax.dot_general(
                query,
                keys_held[seq, head],
                (((1,), (1,)), ((), ())),
                preferred_element_type=F32,
            )
        return carry

    lax.fori_loop(0, rows, score_step, 0, unroll=4)
    chip_collect("ep", half, me, score_land.at[1], score_ss.at[1], score_rs.at[1])
    summed = total_of(score_land.at[1], half).astype(BF16).astype(F32)
    for head in range(heads):
        key_rows[:, head, :] = summed[:, head * size : (head + 1) * size]
    positions = lax.broadcasted_iota(jnp.int32, (rows, heads, span), 2)
    sequences = lax.broadcasted_iota(jnp.int32, (rows, heads, size), 0)
    live_wide = jnp.zeros((rows, heads, size), jnp.int32)
    for seq in range(rows):
        live_wide = jnp.where(sequences == seq, lengths[0, seq], live_wide)
    lives = live_wide[:, :, 0:1]
    gate_all = gates[...]
    last_gate = jnp.sum(jnp.where(positions == lives - 1, gate_all, 0.0), axis=-1, keepdims=True)
    gate_now = last_gate + forget_logs[:, :, 0:1]
    score_all = scores[...] * scale + gate_now - gate_all
    score_all = jnp.where(positions < lives, score_all, -jnp.inf)
    own_score = jnp.sum(query_rows[...] * key_rows[...], axis=-1, keepdims=True) * scale
    row_top = jnp.maximum(jnp.max(score_all, axis=-1, keepdims=True), own_score)
    raised = jnp.exp(score_all - row_top)
    own_raised = jnp.exp(own_score - row_top)
    totals = jnp.sum(raised, axis=-1, keepdims=True) + own_raised
    scores[...] = raised / totals
    own_prob = (own_raised / totals).astype(BF16).astype(F32)

    def value_step(seq, carry):
        for head in range(heads):
            weight = scores[seq, head : head + 1, :].astype(BF16)
            mixed[seq, head : head + 1, :] = dot32(weight, values_held[seq, head])
        return carry

    lax.fori_loop(0, rows, value_step, 0, unroll=4)
    chip_collect("ep", half, me, value_land, value_ss, value_rs)
    value_sum = total_of(value_land, half).astype(BF16).astype(F32)
    for head in range(heads):
        value_rows[:, head, :] = value_sum[:, head * size : (head + 1) * size]
    mixed[...] = mixed[...] + own_prob * value_rows[...]
    for head in range(heads):
        attended[:, head * size : (head + 1) * size] = mixed[:, head, :].astype(BF16)

    sent += fan_out("ep", n_ep, me, lambda t: attended, att_land, att_ss, att_rs)
    att_land[me] = attended[...]
    collect("ep", n_ep, me, att_land, att_ss, att_rs)
    loads[5].wait()
    shares = dot32(att_land[...].reshape(n_ep * rows, hidden), output_weight_held[...])
    head_send[...] = shares.reshape(n_tp, ratio, rows, depth)
    sent += fan_out("tp", n_tp, me_tp, lambda t: head_send.at[t], head_land, head_ss, head_rs)
    head_land[me_tp] = head_send[me_tp]
    collect("tp", n_tp, me_tp, head_land, head_ss, head_rs)
    residual = (token_land[...].astype(F32) + total_of(head_land, n_tp)).astype(BF16)
    res_send[...] = residual
    sent += fan_out("tp", n_tp, me_tp, lambda t: res_send, res_land, res_ss, res_rs)
    for part in range(ratio):
        picked = dot32(dispatch[part], residual[part])
        slot_send[:, part] = picked.reshape(n_ep, slots, depth).astype(BF16)
    sent += fan_out(
        "ep", n_ep, me, lambda t: slot_send.at[t], slot_land.at[me_tp], slot_ss, slot_rs
    )
    slot_land[me_tp, me] = slot_send[me]
    res_land[me_tp] = residual

    def forward(source):
        for step in far_first(n_tp):
            remote(
                slot_land.at[me_tp, source],
                slot_land.at[me_tp, source],
                pass_ss.at[step],
                pass_rs.at[me_tp],
                {"tp": toward(me_tp, step, n_tp)},
            ).start()

    def relay(step):
        source = origin(me, step, n_ep)
        arrive("ep", source, slot_land.at[me_tp, source], slot_ss.at[step], slot_rs.at[source])
        forward(source)

    forward(me)
    early = min(4, n_ep)
    for step in range(1, early):
        relay(step)

    collect("tp", n_tp, me_tp, res_land, res_ss, res_rs)
    held = res_land[...].reshape(n_ep * rows, depth).astype(F32)
    dense_rows = (held * gain_parts[me]).astype(BF16)
    squares = jnp.sum(held * held, axis=-1, keepdims=True)
    mixes = jnp.sum(dense_rows.astype(F32) * mix_parts[me], axis=-1, keepdims=True)
    lane_at = lax.broadcasted_iota(jnp.int32, (n_ep * rows, 128), 1)
    sums = jnp.where(lax.rem(lane_at, 2) == 0, squares, mixes)
    loads[6].wait()
    loads[7].wait()
    products = (
        (0, hidden, dot32(dense_rows, dense_gate_held[...])),
        (hidden, wide, dot32(dense_rows, dense_up_held[...])),
        (wide, wide + 128, sums),
    )
    for start, stop, product in products:
        for place in range(n_ep):
            pair_send[place % 2, place // 2, :, start:stop] = product[
                place * rows : (place + 1) * rows
            ]
    swap = pair_copy("ep", me, pair_send.at[1 - core], pair_land, pair_ss, pair_rs, 0)
    swap.start()
    sent.append(swap)
    owner_copies = row_copies(
        lambda t: res_land.at[t // ratio, lax.rem(t, ratio)], own_land, own_ss, own_rs
    )
    for step in range(early, n_ep):
        relay(step)
    swap.wait_recv()
    paired = pair_send[core] + pair_land[...]
    dense_send[:, :, :wide] = paired[:, :, :wide].astype(BF16)
    tail = paired[:, :, wide:]
    coarse = tail.astype(BF16)
    fine = (tail - coarse.astype(F32)).astype(BF16)
    lane_at = lax.broadcasted_iota(jnp.int32, (half, rows, 128), 2)
    dense_send[:, :, wide:] = jnp.where(
        lane_at < 2, coarse.astype(F32), fine.astype(F32)
    ).astype(BF16)
    sent += chip_fan("ep", half, me, dense_send, dense_land, dense_ss, dense_rs)

    @pl.when(spreads)
    def _():
        for copy in owner_copies:
            copy.start()
        own_land[part_at] = res_land[me // ratio, part_at]

    for step in range(1, n_tp):
        source = origin(me_tp, step, n_tp)
        arrive("tp", source, slot_land.at[source], pass_ss.at[step], pass_rs.at[source])
    total_slots = n_tp * ratio * slots
    square = jnp.zeros((total_slots, depth), F32)
    for index in range(n_ep):
        part = slot_land[:, index].astype(F32).reshape(total_slots, depth)
        square = square + part * part
    slot_scale = lax.rsqrt(jnp.sum(square, axis=-1, keepdims=True) / model + EPSILON)
    for index in range(n_ep):
        part = slot_land[:, index].astype(F32).reshape(total_slots, depth)
        ffn_rows[:, index * depth : (index + 1) * depth] = (
            part * slot_scale * gain_parts[index]
        ).astype(BF16)
    for load in loads[8:]:
        load.wait()
    ffn_in = ffn_rows[...]
    expert_hidden = (
        silu(dot32(ffn_in, expert_gate_held[0])) * dot32(ffn_in, expert_up_held[0])
    ).astype(BF16)
    for step in far_first(n_tp):
        target = toward(me_tp, step, n_tp)
        expert_send[target] = dot32(expert_hidden, expert_down_held[target]).astype(BF16)
        copy = remote(
            expert_send.at[target],
            expert_land.at[me_tp],
            expert_ss.at[step],
            expert_rs.at[me_tp],
            {"tp": target},
        )
        copy.start()
        sent.append(copy)
    expert_land[me_tp] = dot32(expert_hidden, expert_down_held[me_tp]).astype(BF16)

    chip_collect("ep", half, me, dense_land, dense_ss, dense_rs)
    dense_sum = total_of(dense_land, half)
    sums = dense_sum[:, wide:]
    row_scale = lax.rsqrt((sums[:, 0:1] + sums[:, 2:3]) / model + EPSILON)
    mix = jax.nn.sigmoid((sums[:, 1:2] + sums[:, 3:4]) * row_scale)
    dense_pair = dense_sum[:, :wide] * row_scale
    hidden_send[...] = (silu(dense_pair[:, :hidden]) * dense_pair[:, hidden:]).astype(BF16)
    sent += fan_out("ep", n_ep, me, lambda t: hidden_send, hidden_land, hidden_ss, hidden_rs)
    hidden_land[me] = hidden_send[...]

    collect("ep", n_ep, me, hidden_land, hidden_ss, hidden_rs)
    down = dot32(hidden_land[...].reshape(n_ep * rows, hidden), dense_down_held[...])
    tail_send[...] = down.astype(BF16).reshape(n_ep, rows, depth)
    sent += fan_out("ep", n_ep, me, lambda t: tail_send.at[t], tail_land, tail_ss, tail_rs)
    tail_land[me] = tail_send[me]

    collect("tp", n_tp, me_tp, expert_land, expert_ss, expert_rs)
    expert_total = total_of(expert_land, n_tp)
    for index in range(n_ep):
        back_send[index] = expert_total[index * slots : (index + 1) * slots].astype(BF16)
    sent += fan_out("ep", n_ep, me, lambda t: back_send.at[t], back_land, back_ss, back_rs)
    back_land[me] = back_send[me]

    def quarter_copy(source):
        return remote(
            tail_land.at[source],
            quarter_land.at[me_tp, lax.rem(source, ratio)],
            quarter_ss.at[source],
            quarter_rs.at[me_tp, lax.rem(source, ratio)],
            {"tp": source // ratio},
        )

    for step in range(n_ep):
        source = me if step == 0 else origin(me, step, n_ep)
        if step:
            arrive("ep", source, tail_land.at[source], tail_ss.at[step], tail_rs.at[source])

        @pl.when(source // ratio != me_tp)
        def _():
            quarter_copy(source).start()

        @pl.when(source // ratio == me_tp)
        def _():
            quarter_land[me_tp, lax.rem(source, ratio)] = tail_land[source]

    collect("ep", n_ep, me, back_land, back_ss, back_rs)
    back_rows = jnp.concatenate(
        [back_land[index].astype(F32) for index in range(n_ep)], axis=0
    ).astype(BF16)
    route_part[...] = first_route * pick(to_first, back_rows) + second_route * pick(
        to_second, back_rows
    )
    row_arrivals(me_tp, own_land, own_ss, own_rs)
    for step in range(1, n_tp):
        source = origin(me_tp, step, n_tp)
        for part in range(ratio):
            arrive(
                "tp",
                source,
                quarter_land.at[source, part],
                quarter_ss.at[0],
                quarter_rs.at[source, part],
            )
    for part in range(ratio):
        columns = slice(part * depth, (part + 1) * depth)
        out_send[:, columns] = (
            own_land[part].astype(F32)
            + route_part[:, columns]
            + mix * total_of(quarter_land.at[:, part], n_tp)
        ).astype(BF16)
    sent += fan_out("tp", n_tp, me_tp, lambda t: out_send, out_land, out_ss, out_rs)
    out_land[me_tp] = out_send[...]
    for copy in sent[:-1]:
        copy.wait_send()
    for step in range(1, n_tp):
        remote(
            slot_land.at[me_tp],
            slot_land.at[me_tp],
            pass_ss.at[step],
            pass_rs.at[me_tp],
            {"tp": toward(me_tp, step, n_tp)},
        ).wait_send()

    @pl.when(spreads)
    def _():
        for copy in spread_early + owner_copies:
            copy.wait_send()

    for source in range(n_ep):

        @pl.when(source // ratio != me_tp)
        def _():
            quarter_copy(source).wait_send()

    collect("tp", n_tp, me_tp, out_land, out_ss, out_rs)
    for index in range(n_tp):
        out[:, index * chunk : (index + 1) * chunk] = out_land[index]
    sent[-1].wait_send()


def layer(n_ep, n_tp, slots, scalars, small, large):
    rows, model = small[0].shape
    depth, hidden = large[0].shape
    heads, span, size = large[3].shape[1:]
    ratio = n_ep // n_tp
    half = n_ep // 2
    chunk = model // n_tp
    vmem = pl.BlockSpec(memory_space=pltpu.VMEM)
    smem = pl.BlockSpec(memory_space=pltpu.SMEM)
    hbm = pl.BlockSpec(memory_space=pltpu.HBM)
    return pl.pallas_call(
        functools.partial(layer_kernel, n_ep, n_tp),
        out_shape=jax.ShapeDtypeStruct((rows, model), BF16),
        in_specs=[smem] * 2 + [vmem] * len(small) + [hbm] * len(large),
        out_specs=vmem,
        scratch_shapes=[
            pltpu.VMEM(large[0].shape, BF16),
            pltpu.VMEM(large[1].shape, BF16),
            pltpu.VMEM(large[2].shape, BF16),
            pltpu.VMEM(large[3].shape, BF16),
            pltpu.VMEM(large[4].shape, BF16),
            pltpu.VMEM(large[5].shape, BF16),
            pltpu.VMEM(large[6].shape, BF16),
            pltpu.VMEM(large[7].shape, BF16),
            pltpu.VMEM(large[8].shape, BF16),
            pltpu.VMEM(large[9].shape, BF16),
            pltpu.VMEM((n_tp, hidden, chunk), BF16),
            pltpu.VMEM(large[11].shape, BF16),
            pltpu.SemaphoreType.DMA((12 + n_tp,)),
            pltpu.VMEM((n_ep, rows, depth), BF16),
            pltpu.VMEM((n_ep, rows, depth), BF16),
            pltpu.SemaphoreType.DMA((n_ep,)),
            pltpu.SemaphoreType.DMA((n_ep,)),
            pltpu.VMEM((8, 128), F32),
            pltpu.VMEM((ratio, 8, 128), F32),
            pltpu.SemaphoreType.DMA((n_ep,)),
            pltpu.SemaphoreType.DMA((ratio,)),
            pltpu.VMEM((n_ep, rows, depth), BF16),
            pltpu.VMEM((ratio, rows, depth), BF16),
            pltpu.SemaphoreType.DMA((n_ep,)),
            pltpu.SemaphoreType.DMA((ratio,)),
            pltpu.VMEM((3, 2, half, rows, hidden), F32),
            pltpu.VMEM((3, half, rows, hidden), F32),
            pltpu.SemaphoreType.DMA((3,)),
            pltpu.SemaphoreType.DMA((3,)),
            pltpu.VMEM((2, half, rows, hidden), F32),
            pltpu.VMEM((2, half, rows, hidden), F32),
            pltpu.SemaphoreType.DMA((2, half)),
            pltpu.SemaphoreType.DMA((2, half)),
            pltpu.VMEM((half, rows, hidden), BF16),
            pltpu.VMEM((half, rows, hidden), BF16),
            pltpu.SemaphoreType.DMA((half,)),
            pltpu.SemaphoreType.DMA((half,)),
            pltpu.VMEM((rows, heads, size), F32),
            pltpu.VMEM((rows, heads, size), F32),
            pltpu.VMEM((rows, heads, size), F32),
            pltpu.VMEM((rows, heads, size), F32),
            pltpu.VMEM((rows, heads, span), F32),
            pltpu.VMEM((rows, heads, size), F32),
            pltpu.VMEM((rows, hidden), BF16),
            pltpu.VMEM((n_ep, rows, hidden), BF16),
            pltpu.SemaphoreType.DMA((n_ep,)),
            pltpu.SemaphoreType.DMA((n_ep,)),
            pltpu.VMEM((n_tp, ratio, rows, depth), F32),
            pltpu.VMEM((n_tp, ratio, rows, depth), F32),
            pltpu.SemaphoreType.DMA((n_tp,)),
            pltpu.SemaphoreType.DMA((n_tp,)),
            pltpu.VMEM((n_tp, ratio, rows, depth), BF16),
            pltpu.VMEM((ratio, rows, depth), BF16),
            pltpu.SemaphoreType.DMA((n_tp,)),
            pltpu.SemaphoreType.DMA((n_tp,)),
            pltpu.VMEM((ratio, rows, depth), BF16),
            pltpu.SemaphoreType.DMA((n_ep,)),
            pltpu.SemaphoreType.DMA((ratio,)),
            pltpu.VMEM((n_ep, ratio, slots, depth), BF16),
            pltpu.VMEM((n_tp, n_ep, ratio, slots, depth), BF16),
            pltpu.SemaphoreType.DMA((n_ep,)),
            pltpu.SemaphoreType.DMA((n_ep,)),
            pltpu.SemaphoreType.DMA((n_tp,)),
            pltpu.SemaphoreType.DMA((n_tp,)),
            pltpu.VMEM((n_tp * ratio * slots, model), BF16),
            pltpu.VMEM((n_ep, 1, depth), F32),
            pltpu.VMEM((2, half, rows, 2 * hidden + 128), F32),
            pltpu.VMEM((half, rows, 2 * hidden + 128), F32),
            pltpu.SemaphoreType.DMA((1,)),
            pltpu.SemaphoreType.DMA((1,)),
            pltpu.VMEM((half, rows, 2 * hidden + 128), BF16),
            pltpu.VMEM((half, rows, 2 * hidden + 128), BF16),
            pltpu.SemaphoreType.DMA((half,)),
            pltpu.SemaphoreType.DMA((half,)),
            pltpu.VMEM((rows, hidden), BF16),
            pltpu.VMEM((n_ep, rows, hidden), BF16),
            pltpu.SemaphoreType.DMA((n_ep,)),
            pltpu.SemaphoreType.DMA((n_ep,)),
            pltpu.VMEM((n_tp, n_ep * slots, chunk), BF16),
            pltpu.VMEM((n_tp, n_ep * slots, chunk), BF16),
            pltpu.SemaphoreType.DMA((n_tp,)),
            pltpu.SemaphoreType.DMA((n_tp,)),
            pltpu.VMEM((n_ep, slots, chunk), BF16),
            pltpu.VMEM((n_ep, slots, chunk), BF16),
            pltpu.SemaphoreType.DMA((n_ep,)),
            pltpu.SemaphoreType.DMA((n_ep,)),
            pltpu.VMEM((n_ep, rows, depth), BF16),
            pltpu.VMEM((n_ep, rows, depth), BF16),
            pltpu.SemaphoreType.DMA((n_ep,)),
            pltpu.SemaphoreType.DMA((n_ep,)),
            pltpu.VMEM((n_tp, ratio, rows, depth), BF16),
            pltpu.SemaphoreType.DMA((n_ep,)),
            pltpu.SemaphoreType.DMA((n_tp, ratio)),
            pltpu.VMEM((rows, chunk), F32),
            pltpu.VMEM((rows, chunk), BF16),
            pltpu.VMEM((n_tp, rows, chunk), BF16),
            pltpu.SemaphoreType.DMA((n_tp,)),
            pltpu.SemaphoreType.DMA((n_tp,)),
        ],
        compiler_params=pltpu.CompilerParams(
            collective_id=0, has_side_effects=True, vmem_limit_bytes=60 * 1024 * 1024
        ),
    )(*scalars, *small, *large)


def shards(
    tokens,
    attn_gain,
    query_weight,
    key_weight,
    value_weight,
    forget_weight,
    forget_bias,
    cache_keys,
    cache_values,
    cache_gates,
    lengths,
    output_weight,
    ffn_gain,
    dense_gate_proj,
    dense_up_proj,
    dense_down_proj,
    dense_mix,
    expert_ids,
    group_prob,
    pair_prob,
    expert_gate,
    expert_up,
    expert_down,
):
    seq_count = tokens.shape[0]
    n_ep = lax.axis_size("ep")
    n_tp = lax.axis_size("tp")
    expert_count = n_ep * expert_gate.shape[0]
    capacity = max(4 * seq_count // expert_count, 8)
    model = (1, tokens.shape[1])
    return layer(
        n_ep,
        n_tp,
        capacity,
        (forget_bias.reshape(1, -1), lengths.reshape(1, -1)),
        (
            tokens,
            attn_gain.reshape(model),
            forget_weight.T,
            cache_gates,
            ffn_gain.reshape(model),
            ffn_gain.reshape(n_ep, 1, -1),
            dense_mix.reshape(-1, 128),
            expert_ids.T,
            group_prob.reshape(1, -1),
            pair_prob.T,
        ),
        (
            query_weight,
            key_weight,
            value_weight,
            cache_keys,
            cache_values,
            output_weight,
            dense_gate_proj,
            dense_up_proj,
            expert_gate,
            expert_up,
            expert_down,
            dense_down_proj,
        ),
    )


def solution(mesh):
    return jax.shard_map(
        shards,
        mesh=mesh,
        in_specs=(
            P("ep", None),
            P(),
            P("ep", "tp"),
            P("ep", "tp"),
            P("ep", "tp"),
            P(None, "tp"),
            P("tp"),
            P("ep", "tp", None, None),
            P("ep", "tp", None, None),
            P("ep", "tp", None),
            P("ep"),
            P("tp", "ep"),
            P(),
            P("ep", "tp"),
            P("ep", "tp"),
            P("tp", "ep"),
            P(),
            P("ep", None),
            P("ep"),
            P("ep", None),
            P("ep", None, "tp"),
            P("ep", None, "tp"),
            P("ep", "tp", None),
        ),
        out_specs=P("ep", None),
        check_vma=False,
    )
```

time: 71.4 us -> 61 us (0.85)
  Pallas kernels: 69.6 us -> 59.3 us
    pallas_call x1, Pallas kernels: 69.6 us -> 59.3 us  [layer(): pl.pallas_call(functools.partial(layer_kernel, n_ep, n_tp), out_shape=jax...]
where the time goes in v2:
time: 61 us; the launch traced here: 60.8 us
  Pallas kernels  59.3 us (97%)
  local copies, waits for them, and re-layouts  1.47 us (2%)
    pallas_call x1, Pallas kernels, layer(): pl.pallas_call(functools.partial(layer_kernel, n_ep, n_tp), out_shape=jax...  59.3 us
    unnamed x1, local copies, waits for them, and re-layouts  1.47 us

profile of v2, /device:TPU:0, one launch (start us, length us, event | category | flops | bytes accessed | tf_op | source)
XLA Modules:
  0.0 60.8 jit_solution(1833440658975464587)
XLA Ops:
  0.0 59.3 %shard_map.217 = bf16[16,2048]{1,0:T(8,128)(2,1)} custom-call(f32[1,4]{1,0:T(1,128)} %bitcast.17, s32[1,16]{1,0:T(1,128)} %bitcast.18, bf16[16,2048]{1,0:T(8,128)(2,1)} %tokens.1, f32[1,2048]{1,0:T(1,128)} %bitcast.13, bf16[4,2048]{1,0:T(4,128)(2,1)} %bitcast.12, f32[16,4,384]{2,1,0:T(4,128)} %gates.1, f32[1,2048]{1,0:T(1,128)} %bitcast.10, ...), custom_call_target="tpu_custom_call" | custom-call | tf_op jit(solution)/shard_map/pallas_call | solution.py:743
  59.4 1.5 %copy.25 = bf16[16,2048]{1,0:T(8,128)(2,1)} copy(bf16[16,2048]{1,0:T(8,128)(2,1)} %shard_map.217) | data formatting | bytes 131072

commit v3 on v2

v3 whole, which is shorter than its diff:
```python
import functools
import math

import jax
import jax.numpy as jnp
from jax import lax
from jax.experimental import pallas as pl
from jax.experimental.pallas import tpu as pltpu
from jax.sharding import PartitionSpec as P

EPSILON = 1e-06


def rms_scale(values, norm_gain):
    widened = values.astype(jnp.float32)
    return (
        widened
        * lax.rsqrt(jnp.mean(widened * widened, axis=-1, keepdims=True) + EPSILON)
        * norm_gain
    )


MESH = pl.DeviceIdType.MESH
F32 = jnp.float32
BF16 = jnp.bfloat16


def flip(me, step):
    bit = 1
    while bit <= step:
        if step & bit:
            me = me + bit - 2 * bit * lax.rem(me // bit, 2)
        bit *= 2
    return me


def toward(me, step, count):
    return flip(me, step) if count & (count - 1) == 0 else lax.rem(me + step, count)


def origin(me, step, count):
    return flip(me, step) if count & (count - 1) == 0 else lax.rem(me + count - step, count)


def far_first(count):
    return range(count - 1, 0, -1)


def remote(source, place, send_sem, recv_sem, device):
    return pltpu.make_async_remote_copy(
        src_ref=source,
        dst_ref=place,
        send_sem=send_sem,
        recv_sem=recv_sem,
        device_id=device,
        device_id_type=MESH,
    )


def fan_out(axis, count, me, source_of, landing, send_sem, recv_sem):
    copies = []
    for step in far_first(count):
        target = toward(me, step, count)
        copy = remote(
            source_of(target),
            landing.at[me],
            send_sem.at[step],
            recv_sem.at[me],
            {axis: target},
        )
        copy.start()
        copies.append(copy)
    return copies


def arrive(axis, source, place, send_sem, recv_sem):
    remote(place, place, send_sem, recv_sem, {axis: source}).wait_recv()


def collect(axis, count, me, landing, send_sem, recv_sem):
    for step in range(1, count):
        source = origin(me, step, count)
        arrive(axis, source, landing.at[source], send_sem.at[step], recv_sem.at[source])


def total_of(ref, count):
    total = ref[0].astype(F32)
    for index in range(1, count):
        total = total + ref[index].astype(F32)
    return total


def dot32(left, right):
    return jnp.dot(left, right, preferred_element_type=F32)


def silu(values):
    return values / (1.0 + jnp.exp(-values))


def chip_fan(axis, half, me, source_of, landing, send_sem, recv_sem):
    chip, core = me // 2, lax.rem(me, 2)
    copies = []
    for step in far_first(half):
        target = toward(chip, step, half)
        copy = remote(
            source_of(target),
            landing.at[chip],
            send_sem.at[step],
            recv_sem.at[chip],
            {axis: target * 2 + core},
        )
        copy.start()
        copies.append(copy)
    return copies


def chip_collect(axis, half, me, landing, send_sem, recv_sem):
    chip, core = me // 2, lax.rem(me, 2)
    for step in range(1, half):
        source = origin(chip, step, half)
        arrive(
            axis, source * 2 + core, landing.at[source], send_sem.at[step], recv_sem.at[source]
        )


def pick(one_hot, held):
    return lax.dot_general(
        one_hot, held, (((0,), (0,)), ((), ())), preferred_element_type=F32
    )


def slot_tables(ids, experts, slots):
    rows = ids.shape[1]
    row_at = lax.broadcasted_iota(jnp.int32, (rows, rows), 0)
    row_to = lax.broadcasted_iota(jnp.int32, (rows, rows), 1)
    expert_at = lax.broadcasted_iota(jnp.int32, (experts, rows), 0).astype(F32)
    slot_at = lax.broadcasted_iota(jnp.int32, (slots, rows), 0).astype(F32)
    first = ids[0:1, :] == expert_at
    second = ids[1:2, :] == expert_at
    hits = (first | second).astype(F32).astype(BF16)
    earlier = (row_at < row_to).astype(F32).astype(BF16)
    ranks = dot32(hits, earlier)
    tables = []
    for chosen in (first, second):
        place = jnp.where(chosen, ranks, -1.0)
        tables.append(
            jnp.concatenate(
                [
                    (place[expert : expert + 1, :] == slot_at).astype(F32)
                    for expert in range(experts)
                ],
                axis=0,
            )
        )
    return tables


def route_columns(group_prob, pair_prob):
    rows = pair_prob.shape[1]
    row_at = lax.broadcasted_iota(jnp.int32, (rows, rows), 0)
    row_to = lax.broadcasted_iota(jnp.int32, (rows, rows), 1)
    probs = pair_prob[...]
    shares = group_prob[...] * probs / (probs[0:1, :] + probs[1:2, :])
    return [
        jnp.sum(jnp.where(row_at == row_to, shares[k : k + 1, :], 0.0), axis=-1, keepdims=True)
        for k in range(2)
    ]


def layer_kernel(
    n_ep,
    n_tp,
    forget_bias_in,
    lengths_in,
    tokens_in,
    attn_gain_in,
    forget_rows_in,
    gates_in,
    gain_parts_in,
    dense_mix_in,
    expert_ids_in,
    group_prob_in,
    pair_prob_in,
    query_weight,
    key_weight,
    value_weight,
    output_weight,
    dense_gate,
    dense_up,
    dense_down,
    keys,
    values,
    expert_gate,
    expert_up,
    expert_down,
    out,
    forget_bias,
    lengths,
    tokens,
    attn_gain,
    forget_rows,
    gates,
    gain_parts,
    dense_mix,
    expert_ids,
    group_prob,
    pair_prob,
    small_sem,
    query_held,
    key_held,
    value_held,
    output_held,
    dense_gate_held,
    dense_up_held,
    dense_down_held,
    keys_held,
    values_held,
    expert_gate_held,
    expert_up_held,
    expert_down_held,
    load_sem,
    weight_ss,
    weight_rs,
    norm_send,
    norm_land,
    norm_ss,
    norm_rs,
    ids_send,
    ids_land,
    ids_ss,
    ids_rs,
    token_send,
    token_land,
    token_ss,
    token_rs,
    part_kept,
    part_send,
    part_land,
    part_ss,
    part_rs,
    query_rows,
    key_rows,
    value_rows,
    forget_logs,
    scores,
    mixed,
    attended,
    att_land,
    att_ss,
    att_rs,
    head_send,
    head_land,
    head_ss,
    head_rs,
    res_send,
    res_land,
    res_ss,
    res_rs,
    own_land,
    own_ss,
    own_rs,
    slot_send,
    slot_land,
    slot_ss,
    slot_rs,
    pass_ss,
    pass_rs,
    ffn_rows,
    mix_parts,
    dense_send,
    dense_land,
    dense_ss,
    dense_rs,
    hidden_land,
    hidden_send,
    hidden_ss,
    hidden_rs,
    expert_send,
    expert_land,
    expert_ss,
    expert_rs,
    back_send,
    back_land,
    back_ss,
    back_rs,
    tail_send,
    tail_land,
    tail_ss,
    tail_rs,
    out_send,
    out_land,
    out_ss,
    out_rs,
    store_sem,
):
    me = lax.axis_index("ep")
    me_tp = lax.axis_index("tp")
    barrier = pltpu.get_barrier_semaphore()
    half = n_ep // 2
    chip, core = me // 2, lax.rem(me, 2)
    spreads = chip == me_tp

    def greet(axis, mine, count):
        def signal(step, carry):
            pl.semaphore_signal(
                barrier,
                inc=1,
                device_id={axis: lax.rem(mine + step, count)},
                device_id_type=MESH,
            )
            return carry

        lax.fori_loop(1, count, signal, 0, unroll=count <= 8)

    greet("ep", me, n_ep)
    greet("tp", me_tp, n_tp)
    small_loads = [
        pltpu.make_async_copy(source, place, small_sem.at[index])
        for index, (source, place) in enumerate(
            (
                (tokens_in, tokens),
                (attn_gain_in, attn_gain),
                (expert_ids_in, expert_ids),
                (forget_bias_in, forget_bias),
                (forget_rows_in, forget_rows),
                (group_prob_in, group_prob),
                (pair_prob_in, pair_prob),
                (dense_mix_in, dense_mix),
                (gain_parts_in, gain_parts),
                (lengths_in, lengths),
                (gates_in, gates),
            )
        )
    ]
    for load in small_loads:
        load.start()
    rows, model = tokens.shape
    depth, hidden = query_weight.shape
    heads, span, size = keys.shape[1:]
    slots = slot_send.shape[1]
    chunk = model // n_tp
    cols = 2 * depth
    wide = 2 * hidden
    shared = (query_held, key_held, value_held, output_held, dense_gate_held, dense_up_held, dense_down_held)
    sources = [query_weight, key_weight, value_weight, output_weight, dense_gate, dense_up, dense_down, keys, values, expert_gate.at[0], expert_up.at[0]]
    places = [held.at[core] for held in shared]
    places += [keys_held, values_held, expert_gate_held, expert_up_held]
    for index in range(n_tp):
        sources.append(expert_down.at[0, :, pl.ds(index * chunk, chunk)])
        places.append(expert_down_held.at[index])
    loads = [
        pltpu.make_async_copy(source, place, load_sem.at[index])
        for index, (source, place) in enumerate(zip(sources, places))
    ]
    for load in loads[: len(shared)]:
        load.start()
    gifts = [
        remote(
            held.at[core],
            held.at[core],
            weight_ss.at[index],
            weight_rs.at[index],
            {"ep": me + 1 - 2 * core},
        )
        for index, held in enumerate(shared)
    ]

    for load in small_loads[:3]:
        load.wait()
    normed = rms_scale(tokens[...], attn_gain[...])
    for index in range(half):
        norm_send[index] = normed[:, index * cols : (index + 1) * cols].astype(BF16)
        token_send[index] = tokens[:, index * cols : (index + 1) * cols]
    ids = expert_ids[...].astype(F32)
    ids_send[0:2, 0:rows] = ids
    pl.semaphore_wait(barrier, n_ep + n_tp - 2)

    sent = chip_fan("ep", half, me, lambda t: norm_send.at[t], norm_land, norm_ss, norm_rs)
    norm_land[chip] = norm_send[chip]
    for load in loads[len(shared) :]:
        load.start()
    for index in range(len(shared)):
        loads[index].wait()
        gifts[index].start()

    def row_copies(source_of, landing, send_sem, recv_sem):
        return [
            remote(
                source_of(toward(chip, step, half)),
                landing,
                send_sem.at[step],
                recv_sem.at[0],
                {"ep": toward(chip, step, half) * 2 + core},
            )
            for step in far_first(half)
        ]

    def row_arrival(landing, send_sem, recv_sem):
        @pl.when(jnp.logical_not(spreads))
        def _():
            arrive("ep", me_tp * 2 + core, landing, send_sem.at[0], recv_sem.at[0])

    spread_early = row_copies(lambda t: token_send.at[t], token_land, token_ss, token_rs)
    spread_early += row_copies(lambda t: ids_send, ids_land, ids_ss, ids_rs)

    @pl.when(spreads)
    def _():
        for copy in spread_early:
            copy.start()
        token_land[...] = token_send[chip]
        ids_land[...] = ids_send[...]

    chip_collect("ep", half, me, norm_land, norm_ss, norm_rs)
    joined = norm_land[...].reshape(half * rows, cols)
    for index in range(3):
        gifts[index].wait_recv()
        product = dot32(joined, shared[index][...].reshape(cols, hidden)).reshape(
            half, rows, hidden
        )
        part_send[index] = product.astype(BF16)
        sent += chip_fan(
            "ep",
            half,
            me,
            lambda t: part_send.at[index, t],
            part_land.at[index],
            part_ss.at[index],
            part_rs.at[index],
        )
        part_kept[index] = product
    for load in small_loads[3:]:
        load.wait()
    normed_wide = normed.astype(BF16).astype(F32)
    for head in range(heads):
        logit = forget_bias[0, head] + jnp.sum(
            normed_wide * forget_rows[head : head + 1, :].astype(F32), axis=-1, keepdims=True
        )
        forget_log = jnp.minimum(logit, 0.0) - jnp.log1p(jnp.exp(-jnp.abs(logit)))
        forget_logs[:, head, :] = jnp.broadcast_to(forget_log, (rows, size))
    mix_lanes = dense_mix.shape[1]
    mix_wide = dense_mix[...].astype(F32)
    for at in range(0, model, mix_lanes):
        start = at % cols
        mix_parts[at // cols, :, start : start + mix_lanes] = mix_wide[
            at // mix_lanes : at // mix_lanes + 1, :
        ]
    first_table, second_table = slot_tables(ids, n_ep, slots)
    to_first, to_second = first_table.astype(BF16), second_table.astype(BF16)
    first_route, second_route = route_columns(group_prob, pair_prob)
    row_arrival(ids_land, ids_ss, ids_rs)
    tables = slot_tables(ids_land[0:2, 0:rows], n_ep, slots)
    dispatch = (tables[0] + tables[1]).astype(BF16)
    row_arrival(token_land, token_ss, token_rs)

    def reduced(index):
        chip_collect("ep", half, me, part_land.at[index], part_ss.at[index], part_rs.at[index])
        total = part_kept[index, chip]
        for step in range(1, half):
            total = total + part_land[index, origin(chip, step, half)].astype(F32)
        return total.astype(BF16).astype(F32)

    summed = reduced(0)
    for head in range(heads):
        query_rows[:, head, :] = summed[:, head * size : (head + 1) * size]

    scale = 1.0 / math.sqrt(size)
    loads[7].wait()
    loads[8].wait()

    def score_step(seq, carry):
        for head in range(heads):
            query = query_rows[seq, head : head + 1, :].astype(BF16)
            scores[seq, head : head + 1, :] = lax.dot_general(
                query,
                keys_held[seq, head],
                (((1,), (1,)), ((), ())),
                preferred_element_type=F32,
            )
        return carry

    lax.fori_loop(0, rows, score_step, 0, unroll=4)
    summed = reduced(1)
    for head in range(heads):
        key_rows[:, head, :] = summed[:, head * size : (head + 1) * size]
    positions = lax.broadcasted_iota(jnp.int32, (rows, heads, span), 2)
    sequences = lax.broadcasted_iota(jnp.int32, (rows, heads, size), 0)
    live_wide = jnp.zeros((rows, heads, size), jnp.int32)
    for seq in range(rows):
        live_wide = jnp.where(sequences == seq, lengths[0, seq], live_wide)
    lives = live_wide[:, :, 0:1]
    gate_all = gates[...]
    last_gate = jnp.sum(jnp.where(positions == lives - 1, gate_all, 0.0), axis=-1, keepdims=True)
    gate_now = last_gate + forget_logs[:, :, 0:1]
    score_all = scores[...] * scale + gate_now - gate_all
    score_all = jnp.where(positions < lives, score_all, -jnp.inf)
    own_score = jnp.sum(query_rows[...] * key_rows[...], axis=-1, keepdims=True) * scale
    row_top = jnp.maximum(jnp.max(score_all, axis=-1, keepdims=True), own_score)
    raised = jnp.exp(score_all - row_top)
    own_raised = jnp.exp(own_score - row_top)
    totals = jnp.sum(raised, axis=-1, keepdims=True) + own_raised
    scores[...] = raised / totals
    own_prob = (own_raised / totals).astype(BF16).astype(F32)

    def value_step(seq, carry):
        for head in range(heads):
            weight = scores[seq, head : head + 1, :].astype(BF16)
            mixed[seq, head : head + 1, :] = dot32(weight, values_held[seq, head])
        return carry

    lax.fori_loop(0, rows, value_step, 0, unroll=4)
    value_sum = reduced(2)
    for head in range(heads):
        value_rows[:, head, :] = value_sum[:, head * size : (head + 1) * size]
    mixed[...] = mixed[...] + own_prob * value_rows[...]
    for head in range(heads):
        attended[:, head * size : (head + 1) * size] = mixed[:, head, :].astype(BF16)

    sent += chip_fan("ep", half, me, lambda t: attended, att_land, att_ss, att_rs)
    att_land[chip] = attended[...]
    gifts[3].wait_recv()
    chip_collect("ep", half, me, att_land, att_ss, att_rs)
    joined = att_land[...].reshape(half * rows, hidden)
    for side in range(2):
        head_send[:, :, side * depth : (side + 1) * depth] = dot32(
            joined, output_held[side]
        ).reshape(n_tp, rows, depth)
    sent += fan_out("tp", n_tp, me_tp, lambda t: head_send.at[t], head_land, head_ss, head_rs)
    head_land[me_tp] = head_send[me_tp]
    collect("tp", n_tp, me_tp, head_land, head_ss, head_rs)
    residual = (token_land[...].astype(F32) + total_of(head_land, n_tp)).astype(BF16)
    res_send[...] = residual
    sent += fan_out("tp", n_tp, me_tp, lambda t: res_send, res_land, res_ss, res_rs)
    slot_send[...] = dot32(dispatch, residual).reshape(n_ep, slots, cols).astype(BF16)

    def slot_place(source):
        return slot_land.at[me_tp, source // 2, lax.rem(source, 2)]

    for step in far_first(n_ep):
        target = toward(me, step, n_ep)
        copy = remote(
            slot_send.at[target],
            slot_place(me),
            slot_ss.at[step],
            slot_rs.at[me],
            {"ep": target},
        )
        copy.start()
        sent.append(copy)
    slot_land[me_tp, chip, core] = slot_send[me]
    res_land[me_tp] = residual

    def forward(source):
        for step in far_first(n_tp):
            remote(
                slot_place(source),
                slot_place(source),
                pass_ss.at[step],
                pass_rs.at[me_tp],
                {"tp": toward(me_tp, step, n_tp)},
            ).start()

    def relay(step):
        source = origin(me, step, n_ep)
        arrive("ep", source, slot_place(source), slot_ss.at[step], slot_rs.at[source])
        forward(source)

    forward(me)
    early = min(4, n_ep)
    for step in range(1, early):
        relay(step)

    collect("tp", n_tp, me_tp, res_land, res_ss, res_rs)
    held = res_land[...].reshape(half * rows, cols).astype(F32)
    dense_rows = (held * gain_parts[chip]).astype(BF16)
    for index, weight in ((4, dense_gate_held), (5, dense_up_held)):
        gifts[index].wait_recv()
        start = (index - 4) * hidden
        dense_send[:, :, start : start + hidden] = (
            dot32(dense_rows, weight[...].reshape(cols, hidden))
            .reshape(half, rows, hidden)
            .astype(BF16)
        )
    squares = jnp.sum(held * held, axis=-1, keepdims=True)
    mixes = jnp.sum(dense_rows.astype(F32) * mix_parts[chip], axis=-1, keepdims=True)
    lane_at = lax.broadcasted_iota(jnp.int32, (half * rows, 128), 1)
    sums = jnp.where(lax.rem(lane_at, 2) == 0, squares, mixes)
    coarse = sums.astype(BF16).astype(F32)
    dense_send[:, :, wide:] = (
        jnp.where(lane_at < 2, coarse, sums - coarse).astype(BF16).reshape(half, rows, 128)
    )
    sent += chip_fan("ep", half, me, lambda t: dense_send.at[t], dense_land, dense_ss, dense_rs)
    dense_land[chip] = dense_send[chip]
    owner_copies = row_copies(lambda t: res_land.at[t], own_land, own_ss, own_rs)

    @pl.when(spreads)
    def _():
        for copy in owner_copies:
            copy.start()
        own_land[...] = res_land[chip]

    for step in range(early, n_ep):
        relay(step)

    for step in range(1, n_tp):
        source = origin(me_tp, step, n_tp)
        arrive("tp", source, slot_land.at[source], pass_ss.at[step], pass_rs.at[source])
    total_slots = n_ep * slots
    square = jnp.zeros((total_slots, cols), F32)
    for index in range(half):
        part = slot_land[:, index].astype(F32).reshape(total_slots, cols)
        square = square + part * part
    slot_scale = lax.rsqrt(jnp.sum(square, axis=-1, keepdims=True) / model + EPSILON)
    for index in range(half):
        part = slot_land[:, index].astype(F32).reshape(total_slots, cols)
        ffn_rows[:, index * cols : (index + 1) * cols] = (
            part * slot_scale * gain_parts[index]
        ).astype(BF16)
    for load in loads[9:]:
        load.wait()
    ffn_in = ffn_rows[...]
    expert_hidden = (
        silu(dot32(ffn_in, expert_gate_held[...])) * dot32(ffn_in, expert_up_held[...])
    ).astype(BF16)
    chip_collect("ep", half, me, dense_land, dense_ss, dense_rs)
    dense_sum = total_of(dense_land, half)
    sums = dense_sum[:, wide:]
    row_scale = lax.rsqrt((sums[:, 0:1] + sums[:, 2:3]) / model + EPSILON)
    mix = jax.nn.sigmoid((sums[:, 1:2] + sums[:, 3:4]) * row_scale)
    dense_pair = dense_sum[:, :wide] * row_scale
    hidden_send[...] = (silu(dense_pair[:, :hidden]) * dense_pair[:, hidden:]).astype(BF16)
    sent += chip_fan("ep", half, me, lambda t: hidden_send, hidden_land, hidden_ss, hidden_rs)
    hidden_land[chip] = hidden_send[...]

    for step in far_first(n_tp):
        target = toward(me_tp, step, n_tp)
        expert_send[target] = dot32(expert_hidden, expert_down_held[target]).astype(BF16)
        copy = remote(
            expert_send.at[target],
            expert_land.at[me_tp],
            expert_ss.at[step],
            expert_rs.at[me_tp],
            {"tp": target},
        )
        copy.start()
        sent.append(copy)
    expert_land[me_tp] = dot32(expert_hidden, expert_down_held[me_tp]).astype(BF16)

    gifts[6].wait_recv()
    chip_collect("ep", half, me, hidden_land, hidden_ss, hidden_rs)
    joined = hidden_land[...].reshape(half * rows, hidden)
    for side in range(2):
        tail_send[:, :, side * depth : (side + 1) * depth] = (
            dot32(joined, dense_down_held[side]).reshape(half, rows, depth).astype(BF16)
        )

    def tail_copy(target):
        return remote(
            tail_send.at[target],
            tail_land.at[me_tp],
            tail_ss.at[target],
            tail_rs.at[me_tp],
            {"ep": target * 2 + core, "tp": chip},
        )

    for step in range(half - 1, -1, -1):
        target = chip if step == 0 else toward(chip, step, half)
        if step:
            tail_copy(target).start()
        else:
            pl.when(jnp.logical_not(spreads))(lambda: tail_copy(chip).start())

    @pl.when(spreads)
    def _():
        tail_land[me_tp] = tail_send[chip]

    collect("tp", n_tp, me_tp, expert_land, expert_ss, expert_rs)
    expert_total = total_of(expert_land, n_tp)
    for index in range(n_ep):
        back_send[index] = expert_total[index * slots : (index + 1) * slots].astype(BF16)
    sent += fan_out("ep", n_ep, me, lambda t: back_send.at[t], back_land, back_ss, back_rs)
    back_land[me] = back_send[me]
    for copy in gifts:
        copy.wait_send()
    for copy in sent[: -(n_ep - 1)]:
        copy.wait_send()
    for step in range(1, n_tp):
        remote(
            slot_land.at[me_tp],
            slot_land.at[me_tp],
            pass_ss.at[step],
            pass_rs.at[me_tp],
            {"tp": toward(me_tp, step, n_tp)},
        ).wait_send()

    @pl.when(spreads)
    def _():
        for copy in spread_early + owner_copies:
            copy.wait_send()

    row_arrival(own_land, own_ss, own_rs)
    collect("ep", n_ep, me, back_land, back_ss, back_rs)
    back_rows = jnp.concatenate(
        [back_land[index].astype(F32) for index in range(n_ep)], axis=0
    ).astype(BF16)
    partial = (
        own_land[...].astype(F32)
        + first_route * pick(to_first, back_rows)
        + second_route * pick(to_second, back_rows)
    )
    for step in range(n_tp):
        source = me_tp if step == 0 else origin(me_tp, step, n_tp)

        def landed():
            remote(
                tail_land.at[source],
                tail_land.at[source],
                tail_ss.at[0],
                tail_rs.at[source],
                {"ep": me_tp * 2 + core, "tp": source},
            ).wait_recv()

        if step:
            landed()
        else:
            pl.when(jnp.logical_not(spreads))(landed)
    out_send[...] = (partial + mix * total_of(tail_land, n_tp)).astype(BF16)
    last = fan_out("tp", n_tp, me_tp, lambda t: out_send, out_land, out_ss, out_rs)

    def store(index, source):
        return pltpu.make_async_copy(
            source,
            out.at[:, pl.ds(pl.multiple_of(index * chunk, chunk), chunk)],
            store_sem.at[index],
        )

    store(me_tp, out_send).start()
    for copy in sent[-(n_ep - 1) :]:
        copy.wait_send()
    for step in range(half):
        target = chip if step == 0 else toward(chip, step, half)
        if step:
            tail_copy(target).wait_send()
        else:
            pl.when(jnp.logical_not(spreads))(lambda: tail_copy(chip).wait_send())
    for step in range(1, n_tp):
        source = origin(me_tp, step, n_tp)
        arrive("tp", source, out_land.at[source], out_ss.at[step], out_rs.at[source])
        store(source, out_land.at[source]).start()
    for copy in last:
        copy.wait_send()
    for step in range(1, n_tp):
        source = origin(me_tp, step, n_tp)
        store(source, out_land.at[source]).wait()
    store(me_tp, out_send).wait()


def layer(n_ep, n_tp, slots, small, large):
    rows, model = small[2].shape
    mix_shape = small[7].shape
    depth, hidden = large[0].shape
    keys = large[7]
    heads, span, size = keys.shape[1:]
    half = n_ep // 2
    chunk = model // n_tp
    cols = 2 * depth
    if half != n_tp:
        raise ValueError("unsupported mesh")
    hbm = pl.BlockSpec(memory_space=pltpu.HBM)
    return pl.pallas_call(
        functools.partial(layer_kernel, n_ep, n_tp),
        out_shape=jax.ShapeDtypeStruct((rows, model), BF16),
        in_specs=[hbm] * (len(small) + len(large)),
        out_specs=hbm,
        scratch_shapes=[
            pltpu.SMEM((1, heads), F32),
            pltpu.SMEM((1, rows), jnp.int32),
            pltpu.VMEM((rows, model), BF16),
            pltpu.VMEM((1, model), F32),
            pltpu.VMEM((heads, model), BF16),
            pltpu.VMEM((rows, heads, span), F32),
            pltpu.VMEM((half, 1, cols), F32),
            pltpu.VMEM(mix_shape, BF16),
            pltpu.VMEM((2, rows), jnp.int32),
            pltpu.VMEM((1, rows), F32),
            pltpu.VMEM((2, rows), F32),
            pltpu.SemaphoreType.DMA((11,)),
            pltpu.VMEM((2, depth, hidden), BF16),
            pltpu.VMEM((2, depth, hidden), BF16),
            pltpu.VMEM((2, depth, hidden), BF16),
            pltpu.VMEM((2, hidden, depth), BF16),
            pltpu.VMEM((2, depth, hidden), BF16),
            pltpu.VMEM((2, depth, hidden), BF16),
            pltpu.VMEM((2, hidden, depth), BF16),
            pltpu.VMEM(keys.shape, BF16),
            pltpu.VMEM(keys.shape, BF16),
            pltpu.VMEM((model, hidden), BF16),
            pltpu.VMEM((model, hidden), BF16),
            pltpu.VMEM((n_tp, hidden, chunk), BF16),
            pltpu.SemaphoreType.DMA((11 + n_tp,)),
            pltpu.SemaphoreType.DMA((7,)),
            pltpu.SemaphoreType.DMA((7,)),
            pltpu.VMEM((half, rows, cols), BF16),
            pltpu.VMEM((half, rows, cols), BF16),
            pltpu.SemaphoreType.DMA((half,)),
            pltpu.SemaphoreType.DMA((half,)),
            pltpu.VMEM((8, 128), F32),
            pltpu.VMEM((8, 128), F32),
            pltpu.SemaphoreType.DMA((half,)),
            pltpu.SemaphoreType.DMA((1,)),
            pltpu.VMEM((half, rows, cols), BF16),
            pltpu.VMEM((rows, cols), BF16),
            pltpu.SemaphoreType.DMA((half,)),
            pltpu.SemaphoreType.DMA((1,)),
            pltpu.VMEM((3, half, rows, hidden), F32),
            pltpu.VMEM((3, half, rows, hidden), BF16),
            pltpu.VMEM((3, half, rows, hidden), BF16),
            pltpu.SemaphoreType.DMA((3, half)),
            pltpu.SemaphoreType.DMA((3, half)),
            pltpu.VMEM((rows, heads, size), F32),
            pltpu.VMEM((rows, heads, size), F32),
            pltpu.VMEM((rows, heads, size), F32),
            pltpu.VMEM((rows, heads, size), F32),
            pltpu.VMEM((rows, heads, span), F32),
            pltpu.VMEM((rows, heads, size), F32),
            pltpu.VMEM((rows, hidden), BF16),
            pltpu.VMEM((half, rows, hidden), BF16),
            pltpu.SemaphoreType.DMA((half,)),
            pltpu.SemaphoreType.DMA((half,)),
            pltpu.VMEM((n_tp, rows, cols), F32),
            pltpu.VMEM((n_tp, rows, cols), F32),
            pltpu.SemaphoreType.DMA((n_tp,)),
            pltpu.SemaphoreType.DMA((n_tp,)),
            pltpu.VMEM((rows, cols), BF16),
            pltpu.VMEM((n_tp, rows, cols), BF16),
            pltpu.SemaphoreType.DMA((n_tp,)),
            pltpu.SemaphoreType.DMA((n_tp,)),
            pltpu.VMEM((rows, cols), BF16),
            pltpu.SemaphoreType.DMA((half,)),
            pltpu.SemaphoreType.DMA((1,)),
            pltpu.VMEM((n_ep, slots, cols), BF16),
            pltpu.VMEM((n_tp, half, 2, slots, cols), BF16),
            pltpu.SemaphoreType.DMA((n_ep,)),
            pltpu.SemaphoreType.DMA((n_ep,)),
            pltpu.SemaphoreType.DMA((n_tp,)),
            pltpu.SemaphoreType.DMA((n_tp,)),
            pltpu.VMEM((n_ep * slots, model), BF16),
            pltpu.VMEM((half, 1, cols), F32),
            pltpu.VMEM((half, rows, 2 * hidden + 128), BF16),
            pltpu.VMEM((half, rows, 2 * hidden + 128), BF16),
            pltpu.SemaphoreType.DMA((half,)),
            pltpu.SemaphoreType.DMA((half,)),
            pltpu.VMEM((half, rows, hidden), BF16),
            pltpu.VMEM((rows, hidden), BF16),
            pltpu.SemaphoreType.DMA((half,)),
            pltpu.SemaphoreType.DMA((half,)),
            pltpu.VMEM((n_tp, n_ep * slots, chunk), BF16),
            pltpu.VMEM((n_tp, n_ep * slots, chunk), BF16),
            pltpu.SemaphoreType.DMA((n_tp,)),
            pltpu.SemaphoreType.DMA((n_tp,)),
            pltpu.VMEM((n_ep, slots, chunk), BF16),
            pltpu.VMEM((n_ep, slots, chunk), BF16),
            pltpu.SemaphoreType.DMA((n_ep,)),
            pltpu.SemaphoreType.DMA((n_ep,)),
            pltpu.VMEM((half, rows, cols), BF16),
            pltpu.VMEM((n_tp, rows, cols), BF16),
            pltpu.SemaphoreType.DMA((half,)),
            pltpu.SemaphoreType.DMA((n_tp,)),
            pltpu.VMEM((rows, chunk), BF16),
            pltpu.VMEM((n_tp, rows, chunk), BF16),
            pltpu.SemaphoreType.DMA((n_tp,)),
            pltpu.SemaphoreType.DMA((n_tp,)),
            pltpu.SemaphoreType.DMA((n_tp,)),
        ],
        compiler_params=pltpu.CompilerParams(
            collective_id=0, has_side_effects=True, vmem_limit_bytes=60 * 1024 * 1024
        ),
    )(*small, *large)


def shards(
    tokens,
    attn_gain,
    query_weight,
    key_weight,
    value_weight,
    forget_weight,
    forget_bias,
    cache_keys,
    cache_values,
    cache_gates,
    lengths,
    output_weight,
    ffn_gain,
    dense_gate_proj,
    dense_up_proj,
    dense_down_proj,
    dense_mix,
    expert_ids,
    group_prob,
    pair_prob,
    expert_gate,
    expert_up,
    expert_down,
):
    seq_count = tokens.shape[0]
    n_ep = lax.axis_size("ep")
    n_tp = lax.axis_size("tp")
    expert_count = n_ep * expert_gate.shape[0]
    capacity = max(4 * seq_count // expert_count, 8)
    model = (1, tokens.shape[1])
    return layer(
        n_ep,
        n_tp,
        capacity,
        (
            forget_bias.reshape(1, -1),
            lengths.reshape(1, -1),
            tokens,
            attn_gain.reshape(model),
            forget_weight.T,
            cache_gates,
            ffn_gain.reshape(n_ep // 2, 1, -1),
            dense_mix.reshape(-1, 128),
            expert_ids.T,
            group_prob.reshape(1, -1),
            pair_prob.T,
        ),
        (
            query_weight,
            key_weight,
            value_weight,
            output_weight,
            dense_gate_proj,
            dense_up_proj,
            dense_down_proj,
            cache_keys,
            cache_values,
            expert_gate,
            expert_up,
            expert_down,
        ),
    )


def solution(mesh):
    return jax.shard_map(
        shards,
        mesh=mesh,
        in_specs=(
            P("ep", None),
            P(),
            P("ep", "tp"),
            P("ep", "tp"),
            P("ep", "tp"),
            P(None, "tp"),
            P("tp"),
            P("ep", "tp", None, None),
            P("ep", "tp", None, None),
            P("ep", "tp", None),
            P("ep"),
            P("tp", "ep"),
            P(),
            P("ep", "tp"),
            P("ep", "tp"),
            P("tp", "ep"),
            P(),
            P("ep", None),
            P("ep"),
            P("ep", None),
            P("ep", None, "tp"),
            P("ep", None, "tp"),
            P("ep", "tp", None),
        ),
        out_specs=P("ep", None),
        check_vma=False,
    )
```

time: 61 us -> 51.7 us (0.85)
  Pallas kernels: 59.3 us -> 50.1 us
    pallas_call x1, Pallas kernels: 59.3 us -> 50.1 us  [layer(): pl.pallas_call(functools.partial(layer_kernel, n_ep, n_tp), out_shape=jax...]
where the time goes in v3:
time: 51.7 us; the launch traced here: 51.6 us
  Pallas kernels  50.1 us (97%)
  local copies, waits for them, and re-layouts  1.47 us (3%)
    pallas_call x1, Pallas kernels, layer(): pl.pallas_call(functools.partial(layer_kernel, n_ep, n_tp), out_shape=jax...  50.1 us
    unnamed x1, local copies, waits for them, and re-layouts  1.47 us

profile of v3, /device:TPU:0, one launch (start us, length us, event | category | flops | bytes accessed | tf_op | source)
XLA Modules:
  0.0 51.6 jit_solution(2644534645800475664)
XLA Ops:
  0.0 50.1 %shard_map.217 = bf16[16,2048]{1,0:T(8,128)(2,1)} custom-call(f32[1,4]{1,0:T(1,128)} %bitcast.15, s32[1,16]{1,0:T(1,128)} %bitcast.16, bf16[16,2048]{1,0:T(8,128)(2,1)} %tokens_in.1, f32[1,2048]{1,0:T(1,128)} %bitcast.10, bf16[4,2048]{1,0:T(4,128)(2,1)} %bitcast.9, f32[16,4,384]{2,1,0:T(4,128)} %gates_in.1, f32[4,1,512]{2,1,0:T(1,128)} %bitcast.11, ...), custom_call_target="tpu_custom_call" | custom-call | tf_op jit(solution)/shard_map/pallas_call | solution.py:770
  50.1 1.5 %copy.25 = bf16[16,2048]{1,0:T(8,128)(2,1)} copy(bf16[16,2048]{1,0:T(8,128)(2,1)} %shard_map.217) | data formatting | bytes 131072

commit v4 on v3

v4 whole, which is shorter than its diff:
```python
import functools
import math

import jax
import jax.numpy as jnp
from jax import lax
from jax.experimental import pallas as pl
from jax.experimental.pallas import tpu as pltpu
from jax.sharding import PartitionSpec as P

EPSILON = 1e-06


def rms_scale(values, norm_gain):
    widened = values.astype(jnp.float32)
    return (
        widened
        * lax.rsqrt(jnp.mean(widened * widened, axis=-1, keepdims=True) + EPSILON)
        * norm_gain
    )


MESH = pl.DeviceIdType.MESH
F32 = jnp.float32
BF16 = jnp.bfloat16


def flip(me, step):
    bit = 1
    while bit <= step:
        if step & bit:
            me = me + bit - 2 * bit * lax.rem(me // bit, 2)
        bit *= 2
    return me


def toward(me, step, count):
    return flip(me, step) if count & (count - 1) == 0 else lax.rem(me + step, count)


def origin(me, step, count):
    return flip(me, step) if count & (count - 1) == 0 else lax.rem(me + count - step, count)


def far_first(count):
    return range(count - 1, 0, -1)


def remote(source, place, send_sem, recv_sem, device):
    return pltpu.make_async_remote_copy(
        src_ref=source,
        dst_ref=place,
        send_sem=send_sem,
        recv_sem=recv_sem,
        device_id=device,
        device_id_type=MESH,
    )


def batch_of(landing, count, send_sem, recv_sem, device):
    blocks = landing.at[pl.ds(0, count)]
    return remote(blocks, blocks, send_sem.at[0], recv_sem.at[0], device)


def fan_out(axis, count, me, source_of, landing, send_sem, recv_sem):
    for step in far_first(count):
        target = toward(me, step, count)
        remote(
            source_of(target),
            landing.at[me],
            send_sem.at[0],
            recv_sem.at[0],
            {axis: target},
        ).start()
    return batch_of(landing, count - 1, send_sem, recv_sem, {axis: toward(me, 1, count)})


def arrive(axis, source, place, send_sem, recv_sem):
    remote(place, place, send_sem, recv_sem, {axis: source}).wait_recv()


def total_of(ref, count):
    total = ref[0].astype(F32)
    for index in range(1, count):
        total = total + ref[index].astype(F32)
    return total


def dot32(left, right):
    return jnp.dot(left, right, preferred_element_type=F32)


def silu(values):
    return values / (1.0 + jnp.exp(-values))


def chip_fan(axis, half, me, source_of, landing, send_sem, recv_sem):
    chip, core = me // 2, lax.rem(me, 2)
    for step in far_first(half):
        target = toward(chip, step, half)
        remote(
            source_of(target),
            landing.at[chip],
            send_sem.at[0],
            recv_sem.at[0],
            {axis: target * 2 + core},
        ).start()
    return batch_of(
        landing, half - 1, send_sem, recv_sem, {axis: toward(chip, 1, half) * 2 + core}
    )


def pick(one_hot, held):
    return lax.dot_general(
        one_hot, held, (((0,), (0,)), ((), ())), preferred_element_type=F32
    )


def slot_tables(ids, experts, slots):
    rows = ids.shape[1]
    row_at = lax.broadcasted_iota(jnp.int32, (rows, rows), 0)
    row_to = lax.broadcasted_iota(jnp.int32, (rows, rows), 1)
    expert_at = lax.broadcasted_iota(jnp.int32, (experts, rows), 0).astype(F32)
    slot_at = lax.broadcasted_iota(jnp.int32, (slots, rows), 0).astype(F32)
    first = ids[0:1, :] == expert_at
    second = ids[1:2, :] == expert_at
    hits = (first | second).astype(F32).astype(BF16)
    earlier = (row_at < row_to).astype(F32).astype(BF16)
    ranks = dot32(hits, earlier)
    tables = []
    for chosen in (first, second):
        place = jnp.where(chosen, ranks, -1.0)
        tables.append(
            jnp.concatenate(
                [
                    (place[expert : expert + 1, :] == slot_at).astype(F32)
                    for expert in range(experts)
                ],
                axis=0,
            )
        )
    return tables


def route_columns(group_prob, pair_prob):
    rows = pair_prob.shape[1]
    row_at = lax.broadcasted_iota(jnp.int32, (rows, rows), 0)
    row_to = lax.broadcasted_iota(jnp.int32, (rows, rows), 1)
    probs = pair_prob[...]
    shares = group_prob[...] * probs / (probs[0:1, :] + probs[1:2, :])
    return [
        jnp.sum(jnp.where(row_at == row_to, shares[k : k + 1, :], 0.0), axis=-1, keepdims=True)
        for k in range(2)
    ]


def layer_kernel(
    n_ep,
    n_tp,
    forget_bias_in,
    lengths_in,
    tokens_in,
    attn_gain_in,
    forget_rows_in,
    gates_in,
    gain_parts_in,
    dense_mix_in,
    expert_ids_in,
    group_prob_in,
    pair_prob_in,
    query_weight,
    key_weight,
    value_weight,
    output_weight,
    dense_gate,
    dense_up,
    dense_down,
    keys,
    values,
    expert_gate,
    expert_up,
    expert_down,
    out,
    forget_bias,
    lengths,
    tokens,
    attn_gain,
    forget_rows,
    gates,
    gain_parts,
    dense_mix,
    expert_ids,
    group_prob,
    pair_prob,
    small_sem,
    wide_held,
    tall_held,
    keys_held,
    values_held,
    expert_gate_held,
    expert_up_held,
    expert_down_held,
    load_sem,
    weight_ss,
    weight_rs,
    norm_send,
    norm_land,
    norm_ss,
    norm_rs,
    ids_send,
    ids_land,
    ids_ss,
    ids_rs,
    token_send,
    token_land,
    token_ss,
    token_rs,
    part_kept,
    part_send,
    part_land,
    part_ss,
    part_rs,
    query_flat,
    key_flat,
    value_flat,
    forget_flat,
    gate_flat,
    scores,
    mixed,
    attended,
    att_land,
    att_ss,
    att_rs,
    head_send,
    head_land,
    head_ss,
    head_rs,
    res_send,
    res_land,
    res_ss,
    res_rs,
    own_land,
    own_ss,
    own_rs,
    slot_send,
    slot_land,
    slot_ss,
    slot_rs,
    pass_ss,
    pass_rs,
    mix_parts,
    dense_send,
    dense_land,
    dense_ss,
    dense_rs,
    hidden_land,
    hidden_send,
    hidden_ss,
    hidden_rs,
    expert_send,
    expert_land,
    expert_ss,
    expert_rs,
    back_send,
    back_land,
    back_ss,
    back_rs,
    tail_send,
    tail_land,
    tail_ss,
    tail_rs,
    out_send,
    out_land,
    out_ss,
    out_rs,
    store_sem,
):
    me = lax.axis_index("ep")
    me_tp = lax.axis_index("tp")
    barrier = pltpu.get_barrier_semaphore()
    half = n_ep // 2
    chip, core = me // 2, lax.rem(me, 2)
    spreads = chip == me_tp

    def greet(axis, mine, count):
        def signal(step, carry):
            pl.semaphore_signal(
                barrier,
                inc=1,
                device_id={axis: lax.rem(mine + step, count)},
                device_id_type=MESH,
            )
            return carry

        lax.fori_loop(1, count, signal, 0, unroll=count <= 8)

    greet("ep", me, n_ep)
    greet("tp", me_tp, n_tp)
    small_loads = [
        pltpu.make_async_copy(source, place, small_sem.at[index])
        for index, (source, place) in enumerate(
            (
                (tokens_in, tokens),
                (attn_gain_in, attn_gain),
                (expert_ids_in, expert_ids),
                (forget_bias_in, forget_bias),
                (forget_rows_in, forget_rows),
                (group_prob_in, group_prob),
                (pair_prob_in, pair_prob),
                (dense_mix_in, dense_mix),
                (gain_parts_in, gain_parts),
                (lengths_in, lengths),
                (gates_in, gates),
            )
        )
    ]
    for small in small_loads:
        small.start()
    rows, model = tokens.shape
    depth, hidden = query_weight.shape
    heads, span, size = keys.shape[1:]
    slots = slot_send.shape[1]
    chunk = model // n_tp
    cols = 2 * depth
    wide = 2 * hidden
    loads = [
        pltpu.make_async_copy(source, place, load_sem.at[index])
        for source, place, index in (
            (query_weight, wide_held.at[core, 0], 0),
            (key_weight, wide_held.at[core, 1], 0),
            (value_weight, wide_held.at[core, 2], 0),
            (dense_gate, wide_held.at[core, 3], 0),
            (dense_up, wide_held.at[core, 4], 0),
            (output_weight, tall_held.at[core, 0], 1),
            (dense_down, tall_held.at[core, 1], 1),
            (keys, keys_held, 2),
            (values, values_held, 3),
            (expert_gate, expert_gate_held, 4),
            (expert_up, expert_up_held, 5),
        )
    ]
    loads += [
        pltpu.make_async_copy(
            expert_down.at[0, :, pl.ds(index * chunk, chunk)],
            expert_down_held.at[index],
            load_sem.at[6],
        )
        for index in range(n_tp)
    ]
    for load in loads[:7]:
        load.start()

    def loaded(place, index):
        pltpu.make_async_copy(place, place, load_sem.at[index]).wait()

    gifts = [
        remote(
            place,
            place,
            weight_ss.at[index],
            weight_rs.at[index],
            {"ep": me + 1 - 2 * core},
        )
        for index, place in enumerate(
            (
                wide_held.at[core, pl.ds(0, 3)],
                wide_held.at[core, pl.ds(3, 2)],
                tall_held.at[core],
            )
        )
    ]

    for small in small_loads[:3]:
        small.wait()
    normed = rms_scale(tokens[...], attn_gain[...])
    for index in range(half):
        norm_send[index] = normed[:, index * cols : (index + 1) * cols].astype(BF16)
        token_send[index] = tokens[:, index * cols : (index + 1) * cols]
    ids = expert_ids[...].astype(F32)
    ids_send[0, 0:2, 0:rows] = ids
    pl.semaphore_wait(barrier, n_ep + n_tp - 2)

    norm_batch = chip_fan("ep", half, me, lambda t: norm_send.at[t], norm_land, norm_ss, norm_rs)
    sent = [norm_batch]
    norm_land[chip] = norm_send[chip]
    loaded(wide_held.at[core], 0)
    gifts[0].start()
    gifts[1].start()
    for load in loads[7:]:
        load.start()
    loaded(tall_held.at[core], 1)
    gifts[2].start()

    def row_copies(source_of, landing, send_sem, recv_sem):
        return [
            remote(
                source_of(toward(chip, step, half)),
                landing,
                send_sem.at[0],
                recv_sem.at[0],
                {"ep": toward(chip, step, half) * 2 + core},
            )
            for step in far_first(half)
        ]

    def row_arrival(landing, send_sem, recv_sem):
        @pl.when(jnp.logical_not(spreads))
        def _():
            arrive("ep", me_tp * 2 + core, landing, send_sem.at[0], recv_sem.at[0])

    def row_batch(blocks, send_sem, recv_sem):
        other = {"ep": toward(chip, 1, half) * 2 + core}
        return batch_of(blocks, half - 1, send_sem, recv_sem, other)

    spread_early = row_copies(lambda t: token_send.at[t], token_land, token_ss, token_rs)
    spread_early += row_copies(lambda t: ids_send.at[0], ids_land.at[0], ids_ss, ids_rs)

    @pl.when(spreads)
    def _():
        for copy in spread_early:
            copy.start()
        token_land[...] = token_send[chip]
        ids_land[0] = ids_send[0]

    norm_batch.wait_recv()
    gifts[0].wait_recv()
    joined = norm_land[...].reshape(half * rows, cols)
    part_batches = []
    for index in range(3):
        product = dot32(joined, wide_held[:, index].reshape(cols, hidden)).reshape(
            half, rows, hidden
        )
        part_send[index] = product.astype(BF16)
        part_batches.append(
            chip_fan(
                "ep",
                half,
                me,
                lambda t: part_send.at[index, t],
                part_land.at[index],
                part_ss.at[index],
                part_rs.at[index],
            )
        )
        part_kept[index] = product
    sent += part_batches
    for small in small_loads[3:]:
        small.wait()
    normed_wide = normed.astype(BF16).astype(F32)
    for head in range(heads):
        logit = forget_bias[0, head] + jnp.sum(
            normed_wide * forget_rows[head : head + 1, :].astype(F32), axis=-1, keepdims=True
        )
        forget_log = jnp.minimum(logit, 0.0) - jnp.log1p(jnp.exp(-jnp.abs(logit)))
        block = slice(head * rows, (head + 1) * rows)
        forget_flat[block, :] = jnp.broadcast_to(forget_log, (rows, size))
        gate_flat[block, :] = gates[:, head, :]
    mix_lanes = dense_mix.shape[1]
    mix_wide = dense_mix[...].astype(F32)
    for at in range(0, model, mix_lanes):
        start = at % cols
        mix_parts[at // cols, :, start : start + mix_lanes] = mix_wide[
            at // mix_lanes : at // mix_lanes + 1, :
        ]
    first_table, second_table = slot_tables(ids, n_ep, slots)
    to_first, to_second = first_table.astype(BF16), second_table.astype(BF16)
    first_route, second_route = route_columns(group_prob, pair_prob)
    row_arrival(ids_land.at[0], ids_ss, ids_rs)
    tables = slot_tables(ids_land[0][0:2, 0:rows], n_ep, slots)
    dispatch = (tables[0] + tables[1]).astype(BF16)
    row_arrival(token_land, token_ss, token_rs)

    def reduced(index, place):
        part_batches[index].wait_recv()
        total = part_kept[index, chip]
        for step in range(1, half):
            total = total + part_land[index, origin(chip, step, half)].astype(F32)
        total = total.astype(BF16).astype(F32)
        for head in range(heads):
            place[head * rows : (head + 1) * rows, :] = total[:, head * size : (head + 1) * size]

    flat = heads * rows
    scale = 1.0 / math.sqrt(size)
    positions = lax.broadcasted_iota(jnp.int32, (flat, span), 1)
    sequences = lax.broadcasted_iota(jnp.int32, (rows, size), 0)
    live_wide = jnp.zeros((rows, size), jnp.int32)
    for seq in range(rows):
        live_wide = jnp.where(sequences == seq, lengths[0, seq], live_wide)
    lives = jnp.concatenate([live_wide] * heads, axis=0)[:, 0:1]
    gate_all = gate_flat[...]
    last_gate = jnp.sum(jnp.where(positions == lives - 1, gate_all, 0.0), axis=-1, keepdims=True)
    gate_flat[...] = jnp.where(
        positions < lives, last_gate + forget_flat[:, 0:1] - gate_all, -jnp.inf
    )
    loaded(keys_held, 2)
    loaded(values_held, 3)
    reduced(0, query_flat)
    turned = jnp.transpose(query_flat[...]).astype(BF16)
    column = lax.broadcasted_iota(jnp.int32, (size, flat), 1)
    spots = [(head, seq) for head in range(heads) for seq in range(rows)]
    query_wide = jnp.concatenate(
        [
            jnp.where(column == spot, turned.astype(F32), 0.0).astype(BF16)
            for spot in range(flat)
        ],
        axis=0,
    )
    keys_wide = jnp.concatenate([keys_held[seq, head] for head, seq in spots], axis=1)
    score_all = jnp.transpose(dot32(keys_wide, query_wide)) * scale + gate_flat[...]
    reduced(1, key_flat)
    own_score = jnp.sum(query_flat[...] * key_flat[...], axis=-1, keepdims=True) * scale
    row_top = jnp.maximum(jnp.max(score_all, axis=-1, keepdims=True), own_score)
    raised = jnp.exp(score_all - row_top)
    own_raised = jnp.exp(own_score - row_top)
    totals = jnp.sum(raised, axis=-1, keepdims=True) + own_raised
    scores[...] = raised / totals
    own_prob = (own_raised / totals).astype(BF16).astype(F32)

    def value_step(seq, carry):
        for head in range(heads):
            line = pl.ds(head * rows + seq, 1)
            mixed[line, :] = dot32(scores[line, :].astype(BF16), values_held[seq, head])
        return carry

    lax.fori_loop(0, rows, value_step, 0, unroll=4)
    reduced(2, value_flat)
    blended = (mixed[...] + own_prob * value_flat[...]).astype(BF16)
    for head in range(heads):
        attended[:, head * size : (head + 1) * size] = blended[head * rows : (head + 1) * rows]

    att_batch = chip_fan("ep", half, me, lambda t: attended, att_land, att_ss, att_rs)
    att_land[chip] = attended[...]
    gifts[2].wait_recv()
    att_batch.wait_recv()
    joined = att_land[...].reshape(half * rows, hidden)
    for side in range(2):
        head_send[:, :, side * depth : (side + 1) * depth] = dot32(
            joined, tall_held[side, 0]
        ).reshape(n_tp, rows, depth)
    head_batch = fan_out(
        "tp", n_tp, me_tp, lambda t: head_send.at[t], head_land, head_ss, head_rs
    )
    head_land[me_tp] = head_send[me_tp]
    head_batch.wait_recv()
    residual = (token_land[...].astype(F32) + total_of(head_land, n_tp)).astype(BF16)
    res_send[...] = residual
    res_batch = fan_out("tp", n_tp, me_tp, lambda t: res_send, res_land, res_ss, res_rs)
    slot_send[...] = dot32(dispatch, residual).reshape(n_ep, slots, cols).astype(BF16)

    def slot_place(source):
        return slot_land.at[me_tp, source // 2, lax.rem(source, 2)]

    for step in far_first(n_ep):
        target = toward(me, step, n_ep)
        remote(
            slot_send.at[target],
            slot_place(me),
            slot_ss.at[0],
            slot_rs.at[me],
            {"ep": target},
        ).start()
    sent += [att_batch, head_batch, res_batch]
    sent.append(
        batch_of(slot_send, n_ep - 1, slot_ss, slot_rs, {"ep": toward(me, 1, n_ep)})
    )
    slot_land[me_tp, chip, core] = slot_send[me]
    res_land[me_tp] = residual

    def forward(source):
        for step in far_first(n_tp):
            remote(
                slot_place(source),
                slot_place(source),
                pass_ss.at[0],
                pass_rs.at[source // 2],
                {"tp": toward(me_tp, step, n_tp)},
            ).start()

    def relay(step):
        source = origin(me, step, n_ep)
        arrive("ep", source, slot_place(source), slot_ss.at[0], slot_rs.at[source])
        forward(source)

    forward(me)
    res_batch.wait_recv()
    gifts[1].wait_recv()
    held = res_land[...].reshape(half * rows, cols).astype(F32)
    dense_rows = (held * gain_parts[chip]).astype(BF16)
    for index in range(2):
        start = index * hidden
        dense_send[:, :, start : start + hidden] = (
            dot32(dense_rows, wide_held[:, 3 + index].reshape(cols, hidden))
            .reshape(half, rows, hidden)
            .astype(BF16)
        )
    squares = jnp.sum(held * held, axis=-1, keepdims=True)
    mixes = jnp.sum(dense_rows.astype(F32) * mix_parts[chip], axis=-1, keepdims=True)
    lane_at = lax.broadcasted_iota(jnp.int32, (half * rows, 128), 1)
    sums = jnp.where(lax.rem(lane_at, 2) == 0, squares, mixes)
    coarse = sums.astype(BF16).astype(F32)
    dense_send[:, :, wide:] = (
        jnp.where(lane_at < 2, coarse, sums - coarse).astype(BF16).reshape(half, rows, 128)
    )
    dense_batch = chip_fan(
        "ep", half, me, lambda t: dense_send.at[t], dense_land, dense_ss, dense_rs
    )
    dense_land[chip] = dense_send[chip]
    owner_copies = row_copies(lambda t: res_land.at[t], own_land, own_ss, own_rs)

    @pl.when(spreads)
    def _():
        for copy in owner_copies:
            copy.start()
        own_land[...] = res_land[chip]

    for step in range(1, n_ep):
        relay(step)

    def hidden_step():
        dense_batch.wait_recv()
        dense_sum = total_of(dense_land, half)
        sums = dense_sum[:, wide:]
        row_scale = lax.rsqrt((sums[:, 0:1] + sums[:, 2:3]) / model + EPSILON)
        mix = jax.nn.sigmoid((sums[:, 1:2] + sums[:, 3:4]) * row_scale)
        dense_pair = dense_sum[:, :wide] * row_scale
        hidden_send[...] = (silu(dense_pair[:, :hidden]) * dense_pair[:, hidden:]).astype(BF16)
        hidden_batch = chip_fan(
            "ep", half, me, lambda t: hidden_send, hidden_land, hidden_ss, hidden_rs
        )
        hidden_land[chip] = hidden_send[...]
        return mix, hidden_batch

    total_slots = n_ep * slots
    square = jnp.zeros((total_slots, cols), F32)
    gate_part = jnp.zeros((total_slots, hidden), F32)
    up_part = jnp.zeros((total_slots, hidden), F32)
    loaded(expert_gate_held, 4)
    loaded(expert_up_held, 5)
    for step in range(half):
        if step == half - 1:
            mix, hidden_batch = hidden_step()
        source = chip if step == 0 else origin(chip, step, half)
        blocks = slot_land.at[pl.ds(0, n_tp - 1), source]
        remote(
            blocks,
            blocks,
            pass_ss.at[0],
            pass_rs.at[source],
            {"tp": toward(me_tp, 1, n_tp)},
        ).wait_recv()
        part = slot_land[:, source].astype(F32).reshape(total_slots, cols)
        square = square + part * part
        part = (part * gain_parts[source]).astype(BF16)
        gate_part = gate_part + dot32(part, expert_gate_held[source])
        up_part = up_part + dot32(part, expert_up_held[source])
    slot_scale = lax.rsqrt(jnp.sum(square, axis=-1, keepdims=True) / model + EPSILON)
    expert_hidden = (silu(gate_part * slot_scale) * (up_part * slot_scale)).astype(BF16)

    loaded(expert_down_held, 6)
    for step in far_first(n_tp):
        target = toward(me_tp, step, n_tp)
        expert_send[target] = dot32(expert_hidden, expert_down_held[target]).astype(BF16)
        remote(
            expert_send.at[target],
            expert_land.at[me_tp],
            expert_ss.at[0],
            expert_rs.at[0],
            {"tp": target},
        ).start()
    expert_batch = batch_of(
        expert_land, n_tp - 1, expert_ss, expert_rs, {"tp": toward(me_tp, 1, n_tp)}
    )
    expert_land[me_tp] = dot32(expert_hidden, expert_down_held[me_tp]).astype(BF16)

    sent += [dense_batch, hidden_batch, expert_batch]

    hidden_batch.wait_recv()
    joined = hidden_land[...].reshape(half * rows, hidden)
    for side in range(2):
        tail_send[:, :, side * depth : (side + 1) * depth] = (
            dot32(joined, tall_held[side, 1]).reshape(half, rows, depth).astype(BF16)
        )

    def tail_copy(target):
        return remote(
            tail_send.at[target],
            tail_land.at[me_tp],
            tail_ss.at[0],
            tail_rs.at[0],
            {"ep": target * 2 + core, "tp": chip},
        )

    for step in range(half - 1, -1, -1):
        target = chip if step == 0 else toward(chip, step, half)
        if step:
            tail_copy(target).start()
        else:
            pl.when(jnp.logical_not(spreads))(lambda: tail_copy(chip).start())

    @pl.when(spreads)
    def _():
        tail_land[me_tp] = tail_send[chip]

    expert_batch.wait_recv()
    expert_total = total_of(expert_land, n_tp)
    for index in range(n_ep):
        back_send[index] = expert_total[index * slots : (index + 1) * slots].astype(BF16)
    back_batch = fan_out(
        "ep", n_ep, me, lambda t: back_send.at[t], back_land, back_ss, back_rs
    )
    back_land[me] = back_send[me]
    for copy in gifts:
        copy.wait_send()
    for copy in sent:
        copy.wait_send()
    passed = slot_land.at[pl.ds(0, n_tp - 1)]
    remote(
        passed, passed, pass_ss.at[0], pass_rs.at[0], {"tp": toward(me_tp, 1, n_tp)}
    ).wait_send()

    @pl.when(spreads)
    def _():
        row_batch(token_send, token_ss, token_rs).wait_send()
        row_batch(ids_send, ids_ss, ids_rs).wait_send()
        row_batch(res_land, own_ss, own_rs).wait_send()

    row_arrival(own_land, own_ss, own_rs)
    back_batch.wait_recv()
    back_rows = jnp.concatenate(
        [back_land[index].astype(F32) for index in range(n_ep)], axis=0
    ).astype(BF16)
    partial = (
        own_land[...].astype(F32)
        + first_route * pick(to_first, back_rows)
        + second_route * pick(to_second, back_rows)
    )
    def tail_batch(blocks, count):
        return batch_of(blocks, count, tail_ss, tail_rs, {"ep": toward(me, 2, n_ep)})

    for landed, count in ((spreads, half - 1), (jnp.logical_not(spreads), half)):

        @pl.when(landed)
        def _():
            tail_batch(tail_land, count).wait_recv()

    out_send[...] = (partial + mix * total_of(tail_land, n_tp)).astype(BF16)
    out_land[me_tp] = out_send[...]
    out_batch = fan_out("tp", n_tp, me_tp, lambda t: out_send, out_land, out_ss, out_rs)
    back_batch.wait_send()
    for left, count in ((spreads, half - 1), (jnp.logical_not(spreads), half)):

        @pl.when(left)
        def _():
            tail_batch(tail_send, count).wait_send()

    out_batch.wait_recv()
    for index in range(n_tp):
        pltpu.make_async_copy(
            out_land.at[index], out.at[:, pl.ds(index * chunk, chunk)], store_sem.at[0]
        ).start()
    out_batch.wait_send()
    pltpu.make_async_copy(tokens, out, store_sem.at[0]).wait()


def layer(n_ep, n_tp, slots, small, large):
    rows, model = small[2].shape
    mix_shape = small[7].shape
    depth, hidden = large[0].shape
    keys = large[7]
    heads, span, size = keys.shape[1:]
    half = n_ep // 2
    chunk = model // n_tp
    cols = 2 * depth
    if half != n_tp:
        raise ValueError("unsupported mesh")
    hbm = pl.BlockSpec(memory_space=pltpu.HBM)
    return pl.pallas_call(
        functools.partial(layer_kernel, n_ep, n_tp),
        out_shape=jax.ShapeDtypeStruct((rows, model), BF16),
        in_specs=[hbm] * (len(small) + len(large)),
        out_specs=hbm,
        scratch_shapes=[
            pltpu.SMEM((1, heads), F32),
            pltpu.SMEM((1, rows), jnp.int32),
            pltpu.VMEM((rows, model), BF16),
            pltpu.VMEM((1, model), F32),
            pltpu.VMEM((heads, model), BF16),
            pltpu.VMEM((rows, heads, span), F32),
            pltpu.VMEM((half, 1, cols), F32),
            pltpu.VMEM(mix_shape, BF16),
            pltpu.VMEM((2, rows), jnp.int32),
            pltpu.VMEM((1, rows), F32),
            pltpu.VMEM((2, rows), F32),
            pltpu.SemaphoreType.DMA((11,)),
            pltpu.VMEM((2, 5, depth, hidden), BF16),
            pltpu.VMEM((2, 2, hidden, depth), BF16),
            pltpu.VMEM(keys.shape, BF16),
            pltpu.VMEM(keys.shape, BF16),
            pltpu.VMEM((half, cols, hidden), BF16),
            pltpu.VMEM((half, cols, hidden), BF16),
            pltpu.VMEM((n_tp, hidden, chunk), BF16),
            pltpu.SemaphoreType.DMA((7,)),
            pltpu.SemaphoreType.DMA((3,)),
            pltpu.SemaphoreType.DMA((3,)),
            pltpu.VMEM((half, rows, cols), BF16),
            pltpu.VMEM((half, rows, cols), BF16),
            pltpu.SemaphoreType.DMA((1,)),
            pltpu.SemaphoreType.DMA((1,)),
            pltpu.VMEM((half, 8, 128), F32),
            pltpu.VMEM((1, 8, 128), F32),
            pltpu.SemaphoreType.DMA((1,)),
            pltpu.SemaphoreType.DMA((1,)),
            pltpu.VMEM((half, rows, cols), BF16),
            pltpu.VMEM((rows, cols), BF16),
            pltpu.SemaphoreType.DMA((1,)),
            pltpu.SemaphoreType.DMA((1,)),
            pltpu.VMEM((3, half, rows, hidden), F32),
            pltpu.VMEM((3, half, rows, hidden), BF16),
            pltpu.VMEM((3, half, rows, hidden), BF16),
            pltpu.SemaphoreType.DMA((3, 1)),
            pltpu.SemaphoreType.DMA((3, 1)),
            pltpu.VMEM((heads * rows, size), F32),
            pltpu.VMEM((heads * rows, size), F32),
            pltpu.VMEM((heads * rows, size), F32),
            pltpu.VMEM((heads * rows, size), F32),
            pltpu.VMEM((heads * rows, span), F32),
            pltpu.VMEM((heads * rows, span), F32),
            pltpu.VMEM((heads * rows, size), F32),
            pltpu.VMEM((rows, hidden), BF16),
            pltpu.VMEM((half, rows, hidden), BF16),
            pltpu.SemaphoreType.DMA((1,)),
            pltpu.SemaphoreType.DMA((1,)),
            pltpu.VMEM((n_tp, rows, cols), F32),
            pltpu.VMEM((n_tp, rows, cols), F32),
            pltpu.SemaphoreType.DMA((1,)),
            pltpu.SemaphoreType.DMA((1,)),
            pltpu.VMEM((rows, cols), BF16),
            pltpu.VMEM((n_tp, rows, cols), BF16),
            pltpu.SemaphoreType.DMA((1,)),
            pltpu.SemaphoreType.DMA((1,)),
            pltpu.VMEM((rows, cols), BF16),
            pltpu.SemaphoreType.DMA((1,)),
            pltpu.SemaphoreType.DMA((1,)),
            pltpu.VMEM((n_ep, slots, cols), BF16),
            pltpu.VMEM((n_tp, half, 2, slots, cols), BF16),
            pltpu.SemaphoreType.DMA((1,)),
            pltpu.SemaphoreType.DMA((n_ep,)),
            pltpu.SemaphoreType.DMA((1,)),
            pltpu.SemaphoreType.DMA((half,)),
            pltpu.VMEM((half, 1, cols), F32),
            pltpu.VMEM((half, rows, 2 * hidden + 128), BF16),
            pltpu.VMEM((half, rows, 2 * hidden + 128), BF16),
            pltpu.SemaphoreType.DMA((1,)),
            pltpu.SemaphoreType.DMA((1,)),
            pltpu.VMEM((half, rows, hidden), BF16),
            pltpu.VMEM((rows, hidden), BF16),
            pltpu.SemaphoreType.DMA((1,)),
            pltpu.SemaphoreType.DMA((1,)),
            pltpu.VMEM((n_tp, n_ep * slots, chunk), BF16),
            pltpu.VMEM((n_tp, n_ep * slots, chunk), BF16),
            pltpu.SemaphoreType.DMA((1,)),
            pltpu.SemaphoreType.DMA((1,)),
            pltpu.VMEM((n_ep, slots, chunk), BF16),
            pltpu.VMEM((n_ep, slots, chunk), BF16),
            pltpu.SemaphoreType.DMA((1,)),
            pltpu.SemaphoreType.DMA((1,)),
            pltpu.VMEM((half, rows, cols), BF16),
            pltpu.VMEM((n_tp, rows, cols), BF16),
            pltpu.SemaphoreType.DMA((1,)),
            pltpu.SemaphoreType.DMA((1,)),
            pltpu.VMEM((rows, chunk), BF16),
            pltpu.VMEM((n_tp, rows, chunk), BF16),
            pltpu.SemaphoreType.DMA((1,)),
            pltpu.SemaphoreType.DMA((1,)),
            pltpu.SemaphoreType.DMA((1,)),
        ],
        compiler_params=pltpu.CompilerParams(
            collective_id=0, has_side_effects=True, vmem_limit_bytes=60 * 1024 * 1024
        ),
    )(*small, *large)


def shards(
    tokens,
    attn_gain,
    query_weight,
    key_weight,
    value_weight,
    forget_weight,
    forget_bias,
    cache_keys,
    cache_values,
    cache_gates,
    lengths,
    output_weight,
    ffn_gain,
    dense_gate_proj,
    dense_up_proj,
    dense_down_proj,
    dense_mix,
    expert_ids,
    group_prob,
    pair_prob,
    expert_gate,
    expert_up,
    expert_down,
):
    seq_count = tokens.shape[0]
    n_ep = lax.axis_size("ep")
    n_tp = lax.axis_size("tp")
    expert_count = n_ep * expert_gate.shape[0]
    capacity = max(4 * seq_count // expert_count, 8)
    model = (1, tokens.shape[1])
    return layer(
        n_ep,
        n_tp,
        capacity,
        (
            forget_bias.reshape(1, -1),
            lengths.reshape(1, -1),
            tokens,
            attn_gain.reshape(model),
            forget_weight.T,
            cache_gates,
            ffn_gain.reshape(n_ep // 2, 1, -1),
            dense_mix.reshape(-1, 128),
            expert_ids.T,
            group_prob.reshape(1, -1),
            pair_prob.T,
        ),
        (
            query_weight,
            key_weight,
            value_weight,
            output_weight,
            dense_gate_proj,
            dense_up_proj,
            dense_down_proj,
            cache_keys,
            cache_values,
            expert_gate.reshape(n_ep // 2, -1, expert_gate.shape[2]),
            expert_up.reshape(n_ep // 2, -1, expert_up.shape[2]),
            expert_down,
        ),
    )


def solution(mesh):
    return jax.shard_map(
        shards,
        mesh=mesh,
        in_specs=(
            P("ep", None),
            P(),
            P("ep", "tp"),
            P("ep", "tp"),
            P("ep", "tp"),
            P(None, "tp"),
            P("tp"),
            P("ep", "tp", None, None),
            P("ep", "tp", None, None),
            P("ep", "tp", None),
            P("ep"),
            P("tp", "ep"),
            P(),
            P("ep", "tp"),
            P("ep", "tp"),
            P("tp", "ep"),
            P(),
            P("ep", None),
            P("ep"),
            P("ep", None),
            P("ep", None, "tp"),
            P("ep", None, "tp"),
            P("ep", "tp", None),
        ),
        out_specs=P("ep", None),
        check_vma=False,
    )
```

time: 51.7 us -> 47.5 us (0.919)
  Pallas kernels: 50.1 us -> 45.9 us
    pallas_call x1, Pallas kernels: 50.1 us -> 45.9 us  [layer(): pl.pallas_call(functools.partial(layer_kernel, n_ep, n_tp), out_shape=jax...]
where the time goes in v4:
time: 47.5 us; the launch traced here: 47.4 us
  Pallas kernels  45.9 us (97%)
  local copies, waits for them, and re-layouts  1.47 us (3%)
    pallas_call x1, Pallas kernels, layer(): pl.pallas_call(functools.partial(layer_kernel, n_ep, n_tp), out_shape=jax...  45.9 us
    unnamed x1, local copies, waits for them, and re-layouts  1.47 us

profile of v4, /device:TPU:0, one launch (start us, length us, event | category | flops | bytes accessed | tf_op | source)
XLA Modules:
  0.0 47.4 jit_solution(3193191295043187567)
XLA Ops:
  0.0 45.9 %shard_map.217 = bf16[16,2048]{1,0:T(8,128)(2,1)} custom-call(f32[1,4]{1,0:T(1,128)} %bitcast.19, s32[1,16]{1,0:T(1,128)} %bitcast.20, bf16[16,2048]{1,0:T(8,128)(2,1)} %tokens_in.1, f32[1,2048]{1,0:T(1,128)} %bitcast.14, bf16[4,2048]{1,0:T(4,128)(2,1)} %bitcast.13, f32[16,4,384]{2,1,0:T(4,128)} %gates_in.1, f32[4,1,512]{2,1,0:T(1,128)} %bitcast.15, ...), custom_call_target="tpu_custom_call" | custom-call | tf_op jit(solution)/shard_map/pallas_call | solution.py:777
  45.9 1.5 %copy.25 = bf16[16,2048]{1,0:T(8,128)(2,1)} copy(bf16[16,2048]{1,0:T(8,128)(2,1)} %shard_map.217) | data formatting | bytes 131072

commit v5 on v4

--- a/solution.py
+++ b/solution.py
@@ -273,7 +273,6 @@
     out_land,
     out_ss,
     out_rs,
-    store_sem,
 ):
     me = lax.axis_index("ep")
     me_tp = lax.axis_index("tp")
@@ -540,9 +539,11 @@
     head_batch = fan_out(
         "tp", n_tp, me_tp, lambda t: head_send.at[t], head_land, head_ss, head_rs
     )
-    head_land[me_tp] = head_send[me_tp]
     head_batch.wait_recv()
-    residual = (token_land[...].astype(F32) + total_of(head_land, n_tp)).astype(BF16)
+    total = head_send[me_tp]
+    for step in range(1, n_tp):
+        total = total + head_land[origin(me_tp, step, n_tp)]
+    residual = (token_land[...].astype(F32) + total).astype(BF16)
     res_send[...] = residual
     res_batch = fan_out("tp", n_tp, me_tp, lambda t: res_send, res_land, res_ss, res_rs)
     slot_send[...] = dot32(dispatch, residual).reshape(n_ep, slots, cols).astype(BF16)
@@ -755,11 +756,8 @@
 
     out_batch.wait_recv()
     for index in range(n_tp):
-        pltpu.make_async_copy(
-            out_land.at[index], out.at[:, pl.ds(index * chunk, chunk)], store_sem.at[0]
-        ).start()
+        out[:, index * chunk : (index + 1) * chunk] = out_land[index]
     out_batch.wait_send()
-    pltpu.make_async_copy(tokens, out, store_sem.at[0]).wait()
 
 
 def layer(n_ep, n_tp, slots, small, large):
@@ -776,9 +774,9 @@
     hbm = pl.BlockSpec(memory_space=pltpu.HBM)
     return pl.pallas_call(
         functools.partial(layer_kernel, n_ep, n_tp),
-        out_shape=jax.ShapeDtypeStruct((rows, model), BF16),
+        out_shape=pltpu.VMEM((rows, model), BF16),
         in_specs=[hbm] * (len(small) + len(large)),
-        out_specs=hbm,
+        out_specs=pl.BlockSpec(memory_space=pltpu.VMEM),
         scratch_shapes=[
             pltpu.SMEM((1, heads), F32),
             pltpu.SMEM((1, rows), jnp.int32),
@@ -870,7 +868,6 @@
             pltpu.SemaphoreType.DMA((1,)),
             pltpu.VMEM((rows, chunk), BF16),
             pltpu.VMEM((n_tp, rows, chunk), BF16),
-            pltpu.SemaphoreType.DMA((1,)),
             pltpu.SemaphoreType.DMA((1,)),
             pltpu.SemaphoreType.DMA((1,)),
         ],

time: 47.5 us -> 46 us (0.968)
  local copies, waits for them, and re-layouts: 1.47 us -> 0.63 us
  Pallas kernels: 45.9 us -> 45.3 us
    unnamed x1, local copies, waits for them, and re-layouts: 1.47 us -> 0.63 us
    pallas_call x1, Pallas kernels: 45.9 us -> 45.3 us  [layer(): pl.pallas_call(functools.partial(layer_kernel, n_ep, n_tp), out_shape=plt...]
where the time goes in v5:
time: 46 us; the launch traced here: 45.9 us
  Pallas kernels  45.3 us (98%)
  local copies, waits for them, and re-layouts  0.63 us (1%)
    pallas_call x1, Pallas kernels, layer(): pl.pallas_call(functools.partial(layer_kernel, n_ep, n_tp), out_shape=plt...  45.3 us

profile of v5, /device:TPU:0, one launch (start us, length us, event | category | flops | bytes accessed | tf_op | source)
XLA Modules:
  0.0 45.9 jit_solution(10321238514968985155)
XLA Ops:
  0.0 45.3 %shard_map.217 = bf16[16,2048]{1,0:T(8,128)(2,1)S(1)} custom-call(f32[1,4]{1,0:T(1,128)} %bitcast.19, s32[1,16]{1,0:T(1,128)} %bitcast.20, bf16[16,2048]{1,0:T(8,128)(2,1)} %tokens_in.1, f32[1,2048]{1,0:T(1,128)} %bitcast.14, bf16[4,2048]{1,0:T(4,128)(2,1)} %bitcast.13, f32[16,4,384]{2,1,0:T(4,128)} %gates_in.1, f32[4,1,512]{2,1,0:T(1,128)} %bitcast.15, ...), custom_call_target="tpu_custom_call" | custom-call | tf_op jit(solution)/shard_map/pallas_call | solution.py:775
  45.3 0.6 %copy.25 = bf16[16,2048]{1,0:T(8,128)(2,1)} copy(bf16[16,2048]{1,0:T(8,128)(2,1)S(1)} %shard_map.217) | data formatting | bytes 131072
